TPU v7x, 256 devices: a whole 4x4x8 slice. The times are simulated.
256 devices in a mesh: ep: 16 (over y, x), tp: 16 (over z, core).
Axes of the slice: x: 4, y: 4, z: 8, core: 2. Of those that a mesh axis runs over, the one named last changes fastest.
Arguments:
- query_preactivation: bfloat16 [32768, 2048], P('ep', 'tp'), may hold values from -6 to 6
- forget_preactivation: bfloat16 [32768, 2048], P('ep', 'tp'), may hold values from -6 to 6
- value_input_rows: bfloat16 [32768, 1024], P('ep', 'tp'), may hold values from -8 to 8
- output_gate_preactivation: bfloat16 [32768, 1024], P('ep', 'tp'), may hold values from -6 to 6
- forget_floor_gap: float32 [2048], P('tp'), may hold values from 0 to 0.2, as said below
- extra_log_forget: float32 [32768, 16], P('ep', 'tp'), may hold values from -2 to 0
- head_output_gain: float32 [1024], P('tp'), may hold values from 0.1 to 1.9
- mixer_output_weight: bfloat16 [1024, 2048], P(None, 'tp'), may hold values from -0.1875 to 0.1875
- second_batch_tokens: bfloat16 [8192, 2048], P('ep'), may hold values from -6 to 6
- feedforward_norm_gain: float32 [2048], replicated, may hold values from 0.1 to 1.9
- chosen_expert_index: int32 [8192, 2], P('ep'), may hold values from 0 to 15, all different within a row; in each aligned block of 32 rows (0 to 31, 32 to 63, ...) at most 5 rows name the same one
- chosen_expert_weight: float32 [8192, 2], P('ep'), may hold values from 0.1 to 1
- expert_gate_weight: bfloat16 [16, 2048, 7168], P('ep', None, 'tp'), may hold values from -0.125 to 0.125
- expert_up_weight: bfloat16 [16, 2048, 7168], P('ep', None, 'tp'), may hold values from -0.125 to 0.125
- expert_down_weight: bfloat16 [16, 7168, 2048], P('ep', 'tp'), may hold values from -0.0625 to 0.0625
Outputs:
- mixer_output_first: bfloat16 [32768, 2048], P('ep', 'tp')
- moe_out: bfloat16 [8192, 2048], P(('ep', 'tp'))
Inputs may be any that keep to these rules, and one draw needn't show every extreme that they name: `chosen_expert_index`: each row names 2 different experts. In each aligned block of 32 rows (the rows of one device's share) no expert is named by more than 5 rows, and in every draw some expert is named by exactly 5 rows of some block. `forget_floor_gap`: every entry is positive.
All inputs are finite; a program needn't handle non-finite values.
Results may differ from a plain program's by a relative error of at most 0.019.
Values may be sent and summed in bfloat16 or wider, within the bound.
A program may use at most 128 MiB of HBM per device.

v0:
```python
import jax
import jax.numpy as jnp
from jax import lax
from jax.sharding import PartitionSpec as P

KEY_DIM = 128
VAL_DIM = 64
BLOCK_POSITIONS = 64
TOPK = 2


epsilon = 1e-06


def copy_for_each(shard, axis):
    copies = jnp.broadcast_to(shard, (lax.axis_size(axis), *shard.shape))
    return lax.all_to_all(copies, axis, split_axis=0, concat_axis=0, tiled=True)


def all_in_one(shard, axis):
    leaves = jax.tree.leaves(shard)
    sequence = sorted(range(len(leaves)), key=lambda k: -leaves[k].size)
    width = (1, *leaves[sequence[0]].shape)[-1]
    lines = [
        jnp.pad(leaves[k].reshape(-1), (0, -leaves[k].size % width)).reshape(-1, width)
        for k in sequence
    ]
    both, at, found = (copy_for_each(jnp.concatenate(lines), axis), 0, {})
    for k, line in zip(sequence, lines):
        slab = both[:, at : at + len(line)].reshape(len(both), -1)
        found[k] = slab[:, : leaves[k].size].reshape(-1, *leaves[k].shape)
        at += len(line)
    numbers = iter(range(len(leaves)))
    return jax.tree.map(lambda _: found[next(numbers)], shard)


def combined_pairwise(pieces, combine):
    while len(jax.tree.leaves(pieces)[0]) > 1:
        pieces = jax.vmap(combine)(
            *(jax.tree.map(lambda part: part[side::2], pieces) for side in (0, 1))
        )
    return jax.tree.map(lambda part: part[0], pieces)


def carried_in(shard, axis, combine, identity):
    count, here = (lax.axis_size(axis), lax.axis_index(axis))
    passed = jnp.arange(count) < here

    def kept(part, zero, own):
        part = jnp.where(
            passed.reshape(-1, *(1 for _ in own.shape)),
            part.astype(own.dtype),
            jnp.asarray(zero, own.dtype),
        )
        return part

    pieces = all_in_one(
        jax.tree.map(lambda part, kind: part.astype(kind), shard, (jnp.bfloat16, jnp.bfloat16)),
        axis,
    )
    return combined_pairwise(jax.tree.map(kept, pieces, identity, shard), combine)


def combine_states(earlier, later):
    return (earlier[0] * later[0], later[0][..., None] * earlier[1] + later[1])


def norm_rows(tokens, row_gain):
    tokens_float = tokens.astype(jnp.float32)
    factor = lax.rsqrt(jnp.mean(tokens_float * tokens_float, axis=-1, keepdims=True) + epsilon)
    return (tokens_float * factor * row_gain).astype(jnp.bfloat16)


def slot_positions(blocks, experts_all):
    flattened = blocks.reshape(blocks.shape[0], -1)
    onehot = (flattened[..., None] == jnp.arange(experts_all, dtype=jnp.int32)).astype(jnp.int32)
    earlier = jnp.cumsum(onehot, axis=1) - onehot
    return jnp.sum(earlier * onehot, axis=-1).reshape(blocks.shape)


def fill_slots(rows_in, blocks, slot_ids, experts_all, capacity):
    groups = blocks.shape[0]
    sub_rows = blocks.shape[1]
    group_ids = jnp.arange(groups, dtype=jnp.int32)[:, None, None]
    target = (group_ids * experts_all + blocks) * capacity + slot_ids
    sources = jnp.broadcast_to(
        jnp.arange(sub_rows, dtype=jnp.int32)[None, :, None] + group_ids * sub_rows, blocks.shape
    )
    lookup = (
        jnp.full((groups * experts_all * capacity,), -1, jnp.int32)
        .at[target.reshape(-1)]
        .set(sources.reshape(-1))
    )
    gathered = rows_in.reshape(groups * sub_rows, -1)[jnp.maximum(lookup, 0)]
    filled = jnp.where((lookup >= 0)[:, None], gathered, jnp.zeros((), gathered.dtype))
    return filled.reshape(groups, experts_all, capacity, -1)


def on_device(
    query_preactivation,
    forget_preactivation,
    value_input_rows,
    output_gate_preactivation,
    forget_floor_gap,
    extra_log_forget,
    head_output_gain,
    mixer_output_weight,
    second_batch_tokens,
    feedforward_norm_gain,
    chosen_expert_index,
    chosen_expert_weight,
    expert_gate_weight,
    expert_up_weight,
    expert_down_weight,
):
    length = query_preactivation.shape[0]
    device_heads = forget_floor_gap.shape[0] // KEY_DIM
    block_count = length // BLOCK_POSITIONS
    shape_key = (block_count, BLOCK_POSITIONS, device_heads, KEY_DIM)
    queries = jax.nn.silu(query_preactivation.astype(jnp.float32)).reshape(shape_key)
    key_decay_rates = forget_floor_gap.reshape(device_heads, KEY_DIM) * jax.nn.sigmoid(
        -forget_preactivation.astype(jnp.float32)
    ).reshape(shape_key)
    forget_log_factor = (
        jnp.log(1.0 - key_decay_rates)
        + extra_log_forget.reshape(block_count, BLOCK_POSITIONS, device_heads)[..., None]
    )
    values = value_input_rows.astype(jnp.float32).reshape(
        block_count, BLOCK_POSITIONS, device_heads, VAL_DIM
    )
    cumulative_log = jnp.cumsum(forget_log_factor, axis=1)
    block_final_row = cumulative_log[:, -1]
    query_scaled = queries * jnp.exp(cumulative_log - block_final_row[:, None])
    scaled_key_rows = key_decay_rates * jnp.exp(block_final_row[:, None] - cumulative_log)
    scores = jnp.einsum("nthk,nshk->nhts", query_scaled, scaled_key_rows)
    causal_mask = jnp.arange(BLOCK_POSITIONS)[:, None] >= jnp.arange(BLOCK_POSITIONS)[None, :]
    scores = jnp.where(causal_mask, scores, 0.0)
    within = jnp.einsum("nhts,nshv->nthv", scores, values)
    updates = jnp.einsum("nshk,nshv->nhkv", scaled_key_rows, values)
    decays = jnp.exp(block_final_row)
    run_decay, run_state = lax.associative_scan(combine_states, (decays, updates))
    carried = carried_in(
        (run_decay[-1], run_state[-1]),
        "ep",
        combine_states,
        (jnp.ones_like(decays[0]), jnp.zeros_like(updates[0])),
    )
    prior_decay = jnp.concatenate([jnp.ones_like(decays[:1]), run_decay[:-1]], axis=0)
    prior_state = jnp.concatenate([jnp.zeros_like(updates[:1]), run_state[:-1]], axis=0)
    prior_full = prior_state + prior_decay[..., None] * carried[1][None]
    across_blocks = jnp.einsum("nthk,nhkv->nthv", queries * jnp.exp(cumulative_log), prior_full)
    recurrent = (within + across_blocks).reshape(length, device_heads, VAL_DIM)
    factor = lax.rsqrt(jnp.mean(recurrent * recurrent, axis=-1, keepdims=True) + epsilon)
    normed = (recurrent * factor * head_output_gain.reshape(device_heads, VAL_DIM)).reshape(
        length, device_heads * VAL_DIM
    )
    mixed = (normed * jax.nn.silu(output_gate_preactivation.astype(jnp.float32))).astype(
        jnp.bfloat16
    )
    mixer_output_first = jnp.dot(
        lax.all_gather(mixed, "tp", axis=1, tiled=True),
        mixer_output_weight,
        preferred_element_type=jnp.float32,
    ).astype(jnp.bfloat16)
    local_experts = expert_gate_weight.shape[0]
    experts_all = local_experts * lax.axis_size("ep")
    groups = lax.axis_size("tp")
    sub_rows = second_batch_tokens.shape[0] // groups
    capacity = max(2, sub_rows * TOPK * 5 // (4 * experts_all))
    position = lax.axis_index("tp")
    own_routes = lax.dynamic_slice_in_dim(chosen_expert_index, position * sub_rows, sub_rows, 0)
    own_weights = lax.dynamic_slice_in_dim(chosen_expert_weight, position * sub_rows, sub_rows, 0)
    own_slots = slot_positions(own_routes[None], experts_all)[0]
    own_rows = lax.dynamic_slice_in_dim(second_batch_tokens, position * sub_rows, sub_rows, 0)
    outgoing = fill_slots(
        norm_rows(own_rows, feedforward_norm_gain)[None],
        own_routes[None],
        own_slots[None],
        experts_all,
        capacity,
    )[0]
    arrived = lax.all_to_all(outgoing, "ep", split_axis=0, concat_axis=0, tiled=True)
    segment = lax.all_gather(arrived[None], "tp", axis=0, tiled=True)
    shaped = segment.reshape(segment.shape[0], -1, local_experts, capacity, segment.shape[-1])
    gate_part = jnp.einsum(
        "tsecd,edf->tsecf", shaped, expert_gate_weight, preferred_element_type=jnp.float32
    )
    up_part = jnp.einsum(
        "tsecd,edf->tsecf", shaped, expert_up_weight, preferred_element_type=jnp.float32
    )
    hidden = (jax.nn.silu(gate_part) * up_part).astype(jnp.bfloat16)
    rows_each = hidden.shape[1] * hidden.shape[2] * hidden.shape[3]
    product = jnp.einsum(
        "tsecf,efd->tsecd", hidden, expert_down_weight, preferred_element_type=jnp.float32
    )
    summed = lax.psum_scatter(
        product.reshape(rows_each * lax.axis_size("tp"), product.shape[-1]).astype(jnp.bfloat16),
        "tp",
        scatter_dimension=0,
        tiled=True,
    ).astype(jnp.float32)
    to_return = summed.astype(jnp.bfloat16).reshape(-1, local_experts * capacity, summed.shape[-1])
    returned = lax.all_to_all(to_return, "ep", split_axis=0, concat_axis=0, tiled=True)
    results = returned.reshape(experts_all * capacity, -1)
    flat_index = own_routes * capacity + own_slots
    combined = jnp.zeros((sub_rows, results.shape[1]), jnp.float32)
    for ranked in range(TOPK):
        combined = (
            combined
            + results[flat_index[:, ranked]].astype(jnp.float32)
            * own_weights[:, ranked : ranked + 1]
        )
    return (mixer_output_first, combined.astype(jnp.bfloat16))


def solution(mesh):
    placed = (
        P("ep", "tp"),
        P("ep", "tp"),
        P("ep", "tp"),
        P("ep", "tp"),
        P("tp"),
        P("ep", "tp"),
        P("tp"),
        P(None, "tp"),
        P("ep", None),
        P(),
        P("ep", None),
        P("ep", None),
        P("ep", None, "tp"),
        P("ep", None, "tp"),
        P("ep", "tp", None),
    )
    return jax.shard_map(
        on_device,
        mesh=mesh,
        in_specs=placed,
        out_specs=(P("ep", "tp"), P(("ep", "tp"), None)),
        check_vma=False,
    )
```

profile of v0, /device:TPU:1, one launch (start us, length us, event | category | flops | bytes accessed | tf_op | source)
XLA Modules:
  0.0 234.6 jit_solution(4051905095843440140)
XLA Ops:
  7.2 0.9 constant_dynamic-slice_fusion.1
  9.0 0.8 scatter_custom_fusion
  9.8 1.0 fusion.61
  10.9 1.0 fusion.63
  11.9 0.8 gather_fusion
  13.1 17.8 %all_to_all.15 = bf16[16,5,2048]{2,1,0:T(8,128)(2,1)S(1)} all-to-all(bf16[16,5,2048]{2,1,0:T(8,128)(2,1)S(1)} %broadcast_select_fusion), channel_id=1, replica_groups=mesh['ep'=16,'tp'=16] {'ep'}, dimensions={0} | all-to-all | bytes 655360 | tf_op jit(solution)/shard_map/all_to_all | solution.py:182
  30.9 0.9 copy.131
  31.9 0.5 broadcast.311
  32.4 0.7 reduce.14
  33.3 0.3 add_divide_fusion
  33.6 42.5 %all-gather.6.cloned.1.call-done = bf16[256,5,2048]{2,0,1:T(8,128)(2,1)} async-done(((bf16[16,5,2048]{2,0,1:T(8,128)(2,1)}), bf16[256,5,2048]{2,0,1:T(8,128)(2,1)}) %all-gather.6.cloned.1.call-update) | async-done | bytes 5242896 | tf_op jit(solution)/shard_map/all_gather | solution.py:183
  76.1 7.5 %fusion = f32[16,16,5,448]{3,1,2,0:T(8,128)} fusion(bf16[16,16,5,2048]{3,1,0,2:T(8,128)(2,1)} %bitcast.161, bf16[1,2048,448]{1,2,0:T(8,128)(2,1)} %param.28), kind=kOutput, calls=%fused_computation.5 | convolution fusion | flops 2348810240 | bytes 9371648 | tf_op jit(solution)/shard_map/tsecd,edf->tsecf/dot_general | solution.py:188
  83.6 10.4 %convert_bitcast_fusion = bf16[16,16,1,5,2048]{4,1,3,0,2:T(8,128)(2,1)} fusion(bf16[1,448,2048]{2,1,0:T(8,128)(2,1)S(1)} %copy-done, f32[16,16,5,448]{3,1,2,0:T(8,128)} %fusion, bf16[16,16,5,2048]{3,1,0,2:T(8,128)(2,1)} %bitcast.162, bf16[1,2048,448]{1,2,0:T(8,128)(2,1)} %param.27), kind=kOutput, calls=%fused_computation.4 | convolution fusion | flops 4703682560 | bytes 16449536 | tf_op jit(solution)/shard_map/tsecf,efd->tsecd/dot_general | solution.py:193
  94.0 10.3 %copy.134 = bf16[16,16,1,5,2048]{4,3,1,0,2:T(8,128)(2,1)} copy(bf16[16,16,1,5,2048]{4,1,3,0,2:T(8,128)(2,1)} %convert_bitcast_fusion) | data formatting | bytes 10485760 | tf_op jit(solution)/shard_map/convert_element_type | solution.py:197
  104.3 10.0 %convert_element_type.116 = bf16[1280,2048]{1,0:T(8,128)(2,1)} reshape(bf16[16,16,1,5,2048]{4,3,1,0,2:T(8,128)(2,1)} %copy.134) | data formatting | bytes 10485760 | tf_op jit(solution)/shard_map/convert_element_type | solution.py:197
  114.4 0.6 copy-done.12
  115.0 0.8 fusion.37
  116.0 0.5 slice_multiply_fusion.4
  116.5 0.6 fusion.84
  117.5 0.5 reshape.453
  118.0 0.3 convert_multiply_fusion
  118.3 2.3 fusion.30
  120.6 0.4 fusion.42
  121.0 0.4 copy-done.4
  122.3 5.9 %pad.149 = f32[31,1,128,64]{2,3,0,1:T(8,128)} pad(f32[16,1,128,64]{2,3,0,1:T(8,128)S(1)} %add.235, f32[]{:T(128)} %constant.15.clone.1), padding=0_0_1x0_0_0x0_0_0x0_0_0 | pad | bytes 1540100
  128.2 0.8 fusion.71
  129.0 0.9 broadcast_in_dim.57
  129.8 6.6 %all-to-all-start = ((bf16[16,130,64]{1,2,0:T(8,128)(2,1)}), bf16[16,130,64]{1,2,0:T(8,128)(2,1)}, u32[]{:S(2)}, u32[]{:S(2)}) async-start(bf16[16,130,64]{1,2,0:T(8,128)(2,1)} %broadcast_in_dim.57), calls=%async_computation | async-start | bytes 1048576 | tf_op jit(solution)/shard_map/all_to_all | solution.py:17
  136.5 6.1 %pad.73 = f32[32,1,128,64]{2,3,0,1:T(8,128)} pad(f32[16,1,128,64]{2,3,0,1:T(8,128)S(1)} %add.235, f32[]{:T(128)} %constant.15.clone.1), padding=1_0_1x0_0_0x0_0_0x0_0_0 | pad | bytes 1572868 | tf_op jit(solution)/shard_map/pad | solution.py:141
  142.8 0.8 pad_maximum_fusion
  143.7 6.2 %pad.72 = f32[32,1,128,64]{2,3,0,1:T(8,128)S(1)} pad(f32[16,1,128,64]{2,3,0,1:T(8,128)} %pad_maximum_fusion, f32[]{:T(128)} %constant.15.clone.1), padding=0_1_1x0_0_0x0_0_0x0_0_0 | pad | bytes 1572868 | tf_op jit(solution)/shard_map/pad | solution.py:141
  149.9 1.1 slice_add_fusion
  151.0 2.0 convolution_bitcast_fusion
  153.1 1.0 slice.331
  154.5 1.1 select_bitcast_fusion
  155.7 0.5 multiply_reduce_fusion
  156.3 0.6 copy.129
  156.9 0.4 reshape.455
  157.4 0.9 fusion.56
  158.3 0.8 constant_dynamic-slice_fusion
  159.2 16.0 %reduce-scatter.2.cloned.1.call-done = bf16[80,2048]{1,0:T(8,128)(2,1)} async-done(((bf16[1280,2048]{1,0:T(8,128)(2,1)}), bf16[80,2048]{1,0:T(8,128)(2,1)}) %reduce-scatter.2.cloned.1.call-update) | async-done | bytes 327696 | tf_op jit(solution)/shard_map/reduce_scatter | solution.py:196
  175.2 1.9 reshape.461
  177.1 6.3 %all-to-all-start.2 = ((bf16[16,5,2048]{2,1,0:T(8,128)(2,1)}), bf16[16,5,2048]{2,1,0:T(8,128)(2,1)S(1)}, u32[]{:S(2)}, u32[]{:S(2)}) async-start(bf16[16,5,2048]{2,1,0:T(8,128)(2,1)} %reshape.461), calls=%async_computation.3 | async-start | bytes 1048576 | tf_op jit(solution)/shard_map/all_to_all | solution.py:203
  183.4 38.0 %all-gather.4.cloned.1.call-done = bf16[2048,1024]{0,1:T(8,128)(2,1)} async-done(((bf16[2048,64]{0,1:T(8,128)(2,1)}), bf16[2048,1024]{0,1:T(8,128)(2,1)}) %all-gather.4.cloned.1.call-update) | async-done | bytes 4194320 | tf_op jit(solution)/shard_map/all_gather | solution.py:161
  221.4 4.4 %convolution_convert_fusion = bf16[2048,128]{1,0:T(8,128)(2,1)} fusion(bf16[2048,1024]{0,1:T(8,128)(2,1)} %all-gather.4.cloned.1.call-done, bf16[1024,128]{1,0:T(8,128)(2,1)S(1)} %copy-done.16), kind=kOutput, calls=%fused_computation.16 | convolution fusion | flops 537133056 | bytes 4980736 | tf_op jit(solution)/shard_map/dot_general | solution.py:160
  226.0 0.7 gather_fusion.1
  226.6 0.7 gather_fusion.2
  227.3 0.8 add_convert_fusion
  (156 shorter events, 4.1 us)
Async XLA Ops:
  7.2 76.4 %copy-start = (bf16[1,448,2048]{2,1,0:T(8,128)(2,1)S(1)}, bf16[1,448,2048]{2,1,0:T(8,128)(2,1)}, u32[]{:S(2)}) copy-start(bf16[1,448,2048]{2,1,0:T(8,128)(2,1)} %param.29) | copy-start | bytes 5505028
  7.2 68.9 %all-gather.6.cloned.1.call-start = ((), (), s32[]{:S(2)}) async-start(), calls=%async_computation.6 | async-start | bytes 5570560 | tf_op jit(solution)/shard_map/all_gather | solution.py:183
  12.7 19.7 %copy-start.11 = (f32[2048,1]{0,1:T(1,128)S(1)}, f32[2048,1]{0,1:T(1,128)}, u32[]{:S(2)}) copy-start(f32[2048,1]{0,1:T(1,128)} %param.20) | copy-start | bytes 24580
  12.7 20.5 %copy-start.7 = (bf16[2048,128]{1,0:T(8,128)(2,1)S(1)}, bf16[2048,128]{1,0:T(8,128)(2,1)}, u32[]{:S(2)}) copy-start(bf16[2048,128]{1,0:T(8,128)(2,1)} %param.16) | copy-start | bytes 1572868
  31.9 143.3 %reduce-scatter.2.cloned.1.call-start = ((), (), s32[]{:S(2)}) async-start(), calls=%async_computation.5 | async-start | bytes 5570560 | tf_op jit(solution)/shard_map/reduce_scatter | solution.py:196
  114.3 0.7 copy-start.12
  114.3 3.2 %copy-start.9 = (bf16[2048,64]{0,1:T(8,128)(2,1)S(1)}, bf16[2048,64]{0,1:T(8,128)(2,1)}, u32[]{:S(2)}) copy-start(bf16[2048,64]{0,1:T(8,128)(2,1)} %param.17) | copy-start | bytes 786436
  114.3 3.7 %copy-start.8 = (bf16[2048,128]{1,0:T(8,128)(2,1)S(1)}, bf16[2048,128]{1,0:T(8,128)(2,1)}, u32[]{:S(2)}) copy-start(bf16[2048,128]{1,0:T(8,128)(2,1)} %param.15) | copy-start | bytes 1572868
  118.0 2.6 %copy-start.6 = (bf16[32,64,64]{1,0,2:T(8,128)(2,1)}, bf16[32,64,64]{1,0,2:T(8,128)(2,1)S(1)}, u32[]{:S(2)}) copy-start(bf16[32,64,64]{1,0,2:T(8,128)(2,1)S(1)} %reshape.453) | copy-start | bytes 786436
  120.6 0.8 copy-start.4
  120.6 1.0 copy-start.13
  120.6 1.0 copy-start.14
  129.8 23.2 %all-to-all-start = ((bf16[16,130,64]{1,2,0:T(8,128)(2,1)}), bf16[16,130,64]{1,2,0:T(8,128)(2,1)}, u32[]{:S(2)}, u32[]{:S(2)}) async-start(bf16[16,130,64]{1,2,0:T(8,128)(2,1)} %broadcast_in_dim.57), calls=%async_computation | async-start | bytes 1048576 | tf_op jit(solution)/shard_map/all_to_all | solution.py:17
  136.4 85.0 %all-gather.4.cloned.1.call-start = ((), (), s32[]{:S(2)}) async-start(), calls=%async_computation.4 | async-start | bytes 4456448 | tf_op jit(solution)/shard_map/all_gather | solution.py:161
  142.8 7.1 %copy-start.2 = (f32[32,1,128,64]{2,3,0,1:T(8,128)S(1)}, f32[32,1,128,64]{2,3,0,1:T(8,128)}, u32[]{:S(2)}) copy-start(f32[32,1,128,64]{2,3,0,1:T(8,128)} %pad.73) | copy-start | bytes 3145732
  142.8 8.2 %copy-start.5 = (bf16[32,64,128]{2,0,1:T(8,128)(2,1)S(1)}, bf16[32,64,128]{2,0,1:T(8,128)(2,1)}, u32[]{:S(2)}) copy-start(bf16[32,64,128]{2,0,1:T(8,128)(2,1)} %copy-done.4) | copy-start | bytes 1572868
  151.0 4.7 %copy-start.3 = (f32[31,1,128,64]{2,3,0,1:T(8,128)S(1)}, f32[31,1,128,64]{2,3,0,1:T(8,128)}, u32[]{:S(2)}) copy-start(f32[31,1,128,64]{2,3,0,1:T(8,128)} %slice_add_fusion) | copy-start | bytes 3047428
  156.2 1.1 copy-start.10
  156.3 1.1 copy-start.15
  156.9 64.5 %copy-start.16 = (bf16[1024,128]{1,0:T(8,128)(2,1)S(1)}, bf16[1024,128]{1,0:T(8,128)(2,1)}, u32[]{:S(2)}) copy-start(bf16[1024,128]{1,0:T(8,128)(2,1)} %param.22) | copy-start | bytes 786436
  177.1 48.7 %all-to-all-start.2 = ((bf16[16,5,2048]{2,1,0:T(8,128)(2,1)}), bf16[16,5,2048]{2,1,0:T(8,128)(2,1)S(1)}, u32[]{:S(2)}, u32[]{:S(2)}) async-start(bf16[16,5,2048]{2,1,0:T(8,128)(2,1)} %reshape.461), calls=%async_computation.3 | async-start | bytes 1048576 | tf_op jit(solution)/shard_map/all_to_all | solution.py:203
  221.4 6.7 %copy-start.1 = (bf16[1,448,2048]{2,1,0:T(8,128)(2,1)S(1)}, bf16[1,448,2048]{2,1,0:T(8,128)(2,1)}, u32[]{:S(2)}) copy-start(bf16[1,448,2048]{2,1,0:T(8,128)(2,1)} %param.29) | copy-start | bytes 5505028
Sparse Core Ops, SparseCore 0:
  32.0 44.0 all-gather.5
  114.5 60.6 reduce-scatter.1
  177.6 43.7 all-gather.3
where the time goes:
time: 236 us; the launch traced here: 235 us
  waiting for transfers between devices  96.6 us (41%)
  local copies, waits for them, and re-layouts  53.1 us (22%)
  matrix products  25.2 us (11%)
  blocking collectives  17.8 us (8%)
  between operations  14.5 us (6%)
  other arithmetic  14.4 us (6%)
  starting transfers between devices  13 us (6%)
    all_gather x1, waiting for transfers between devices, on_device(): segment = lax.all_gather(arrived[None], 'tp', axis=0, tiled=True)  42.5 us
    all_gather x1, waiting for transfers between devices, on_device(): lax.all_gather(mixed, 'tp', axis=1, tiled=True)  38 us
    convert_element_type x2, local copies, waits for them, and re-layouts, on_device(): product.reshape(rows_each * lax.axis_size('tp'), product.shape[-1])  20.4 us
    all_to_all x1, blocking collectives, on_device(): lax.all_to_all(outgoing, 'ep', split_axis=0, concat_axis=0, tiled=True)  17.8 us
    reduce_scatter x1, waiting for transfers between devices, on_device(): lax.psum_scatter(product.reshape(rows_each * lax.axis_size('tp'), product...  16 us
    pad x16, local copies, waits for them, and re-layouts, on_device(): lax.associative_scan(combine_states, (decays, updates))  12.7 us
    dot_general x1, matrix products, on_device(): jnp.einsum('tsecf,efd->tsecd', hidden, expert_down_weight, preferred_elem...  10.4 us
    unnamed x39, local copies, waits for them, and re-layouts  7.75 us
  transfers between devices with their start and end apart: 5, of which 3 were waited for; matrix products, arithmetic and copies ran while one was open for 19% of the time, Pallas kernels for 0%

commit v1 on v0

v1 whole, which is shorter than its diff:
```python
import functools

import jax
import jax.numpy as jnp
from jax import lax
from jax.experimental import pallas as pl
from jax.experimental.pallas import tpu as pltpu
from jax.sharding import PartitionSpec as P

KEY_DIM = 128
VAL_DIM = 64
BLOCK = 64
PAIR = 128
TOPK = 2
EPS = 1e-06
MESH = pl.DeviceIdType.MESH
F32 = jnp.float32
BF16 = jnp.bfloat16
NT = (((1,), (1,)), ((), ()))


def offsets(experts):
    if experts == 16:
        return [
            (0, 0), (0, 1), (3, 0), (0, 3),
            (1, 0), (1, 1), (3, 3), (1, 3),
            (3, 1), (0, 2), (2, 0), (1, 2),
            (2, 3), (3, 2), (2, 1), (2, 2),
        ]
    return [(0, k) for k in range(experts)]


def moved(me, step, experts, back=False):
    dy, dx = step
    if experts != 16:
        return lax.rem(me + (experts - dx if back else dx), experts)
    y, x = me // 4, lax.rem(me, 4)
    if back:
        dy, dx = (4 - dy) % 4, (4 - dx) % 4
    return lax.rem(y + dy, 4) * 4 + lax.rem(x + dx, 4)


def kernel(
    cfg,
    q_hbm, f_hbm, v_hbm, o_hbm, gap_ref, extra_ref, hgain_ref, wo_hbm,
    x_hbm, fgain_ref, idx_ref, wt_ref, wg_hbm, wu_hbm, wd_hbm,
    out_hbm, moe_ref,
    q_s, f_s, v_s, o_s, wo_s, x_s, wg_s, wu_s, wd_s,
    tri_s, dec_s, pre_s, yw_s, qe_s, cs_s, cr_s,
    n_s, slot_s, g_s, s_s, r_s, hid_s, pp_s, qb_s, rb_s,
    m_s, out_s, fs_s, rr_s, gh_s, gl_s, co_s, fo_s,
    lsem, osem, asend, arecv, fsend, frecv, csend, crecv,
    msend, mrecv, dsend, drecv, psend, precv, bsend, brecv, rsend, rrecv, zsend, zrecv,
):
    E, TP, TOK, SUB, CAP = cfg["E"], cfg["TP"], cfg["TOK"], cfg["SUB"], cfg["CAP"]
    Z = TP // 2
    KR = TP * CAP
    KG = max(1, E // 4)
    NG = E // KG
    GR = KG * KR
    D = x_hbm.shape[1]
    H = D // 2
    NTOK = x_hbm.shape[0]
    offs = offsets(E)
    me = lax.axis_index("ep")
    t = lax.axis_index("tp")
    z, c = t // 2, lax.rem(t, 2)
    pc = 1 - c

    def remote(src, dst, ss, rs, e, tt):
        return pltpu.make_async_remote_copy(
            src_ref=src, dst_ref=dst, send_sem=ss, recv_sem=rs, device_id=(e, tt), device_id_type=MESH
        )

    loads = [
        (x_hbm.at[:, 0:H], x_s.at[0]), (x_hbm.at[:, H:D], x_s.at[1]),
        (f_hbm, f_s), (q_hbm, q_s), (v_hbm, v_s), (o_hbm, o_s),
        (wg_hbm, wg_s), (wu_hbm, wu_s), (wd_hbm, wd_s), (wo_hbm, wo_s),
    ]
    loads = [pltpu.make_async_copy(a, b, lsem.at[i]) for i, (a, b) in enumerate(loads)]
    for load in loads:
        load.start()
    barrier = pltpu.get_barrier_semaphore()
    for k in range(1, E):
        pl.semaphore_signal(barrier, inc=1, device_id=(moved(me, offs[k], E), t), device_id_type=MESH)
    for j in range(1, TP):
        pl.semaphore_signal(barrier, inc=1, device_id=(me, lax.rem(t + j, TP)), device_id_type=MESH)

    i0, i1 = idx_ref[0:1, :], idx_ref[1:2, :]
    row_e = lax.broadcasted_iota(jnp.int32, (E, NTOK), 0)
    expert_of = jnp.zeros((E, NTOK), jnp.int32)
    for k in range(E):
        expert_of = jnp.where(row_e == k, moved(me, offs[k], E), expert_of)
    first, second = expert_of == i0, expert_of == i1
    chosen = jnp.where(first | second, 1.0, 0.0)
    ra = lax.broadcasted_iota(jnp.int32, (NTOK, NTOK), 0)
    rb = lax.broadcasted_iota(jnp.int32, (NTOK, NTOK), 1)
    before = jnp.where((ra // SUB == rb // SUB) & (ra < rb), 1.0, 0.0).astype(BF16)
    place = jnp.dot(chosen.astype(BF16), before, preferred_element_type=F32)
    block_of = (lax.broadcasted_iota(jnp.int32, (E, NTOK), 1) // SUB).astype(F32)
    slot_s[...] = jnp.where(chosen > 0, CAP * block_of + place, -1.0)
    weight = jnp.where(first, wt_ref[0:1, :], 0.0) + jnp.where(second, wt_ref[1:2, :], 0.0)
    weight_hi = weight.astype(BF16)
    weight_lo = (weight - weight_hi.astype(F32)).astype(BF16)

    loads[0].wait()
    loads[1].wait()
    gain_half = fgain_ref[:, pl.ds(pl.multiple_of(c * H, 128), H)]

    def norm_rows(i, carry):
        rows = pl.ds(pl.multiple_of(i * 64, 64), 64)
        a, b = x_s[0, rows, :].astype(F32), x_s[1, rows, :].astype(F32)
        total = jnp.sum(a * a + b * b, axis=-1, keepdims=True)
        factor = lax.rsqrt(total / D + EPS)
        n_s[rows, :] = (x_s[c, rows, :].astype(F32) * factor * gain_half).astype(BF16)
        return carry

    lax.fori_loop(0, NTOK // 64, norm_rows, 0)

    place_row = lax.broadcasted_iota(jnp.int32, (KR, NTOK), 0).astype(F32)

    def fill_group(g):
        for k in range(g * KG, (g + 1) * KG):
            rows = slice(k * KR, (k + 1) * KR)
            g_s[rows, :] = jnp.where(place_row == slot_s[k : k + 1, :], 1.0, 0.0).astype(BF16)
        rows = slice(g * GR, (g + 1) * GR)
        pick = g_s[rows, :]
        for n in range(0, H, 256):
            s_s[rows, n : n + 256] = jnp.dot(
                pick, n_s[:, n : n + 256], preferred_element_type=F32
            ).astype(BF16)

    def dispatch(k):
        rows = slice(k * KR, (k + 1) * KR)
        return remote(
            s_s.at[rows, :], r_s.at[c, rows, :], asend.at[k], arecv.at[k], moved(me, offs[k], E), t
        )

    def forward(k):
        rows = slice(k * KR, (k + 1) * KR)
        return remote(
            r_s.at[c, rows, :], r_s.at[c, rows, :], fsend.at[k], frecv.at[k], me, z * 2 + pc
        )

    fill_group(0)
    r_s[c, 0:KR, :] = s_s[0:KR, :]
    pl.semaphore_wait(barrier, E - 1 + TP - 1)
    for k in range(1, KG):
        dispatch(k).start()

    ta = lax.broadcasted_iota(jnp.int32, (PAIR, PAIR), 0)
    tb = lax.broadcasted_iota(jnp.int32, (PAIR, PAIR), 1)
    tri = (ta // BLOCK == tb // BLOCK) & (ta >= tb)
    tri_s[...] = jnp.where(tri, 1.0, 0.0)
    gap = gap_ref[...]
    for load in loads[2:6]:
        load.wait()
    U1 = min(4, TOK // PAIR)

    def local_pairs(i, carry):
        state, decay = carry
        trif = tri_s[...]
        trib = trif.astype(BF16)
        in_first = lax.broadcasted_iota(jnp.int32, (PAIR, PAIR), 0) < BLOCK
        left = lax.broadcasted_iota(jnp.int32, (BLOCK, PAIR), 1) < BLOCK
        later = lax.broadcasted_iota(jnp.int32, (PAIR, PAIR), 1)
        earlier = lax.broadcasted_iota(jnp.int32, (PAIR, PAIR), 0)
        maskt = (later // BLOCK == earlier // BLOCK) & (earlier <= later)
        at = [pl.multiple_of((i * U1 + u) * PAIR, PAIR) for u in range(U1)]
        keys, cums = [], []
        for u in range(U1):
            gate = f_s[pl.ds(at[u], PAIR), :].astype(F32)
            key = gap * (1.0 / (1.0 + jnp.exp(gate)))
            logf = jnp.log(1.0 - key)
            hi = logf.astype(BF16)
            lo = (logf - hi.astype(F32)).astype(BF16)
            cum = jnp.dot(trib, hi, preferred_element_type=F32) + jnp.dot(
                trib, lo, preferred_element_type=F32
            )
            extra = jnp.sum(trif * extra_ref[:, pl.ds(at[u], PAIR)], axis=-1, keepdims=True)
            keys.append(key)
            cums.append(cum + extra)
        work = []
        for u in range(U1):
            key, cum = keys[u], cums[u]
            mid0, mid1 = cum[31:32, :], cum[95:96, :]
            end0, end1 = cum[63:64, :], cum[127:128, :]
            away = cum - jnp.where(in_first, mid0, mid1)
            query = q_s[pl.ds(at[u], PAIR), :].astype(F32)
            query = query * (1.0 / (1.0 + jnp.exp(-query)))
            qs = query * jnp.exp(away)
            ks = key * jnp.exp(-away)
            qe = qs * jnp.where(in_first, jnp.exp(mid0), jnp.exp(mid1))
            ke = ks * jnp.where(in_first, jnp.exp(end0 - mid0), jnp.exp(end1 - mid1))
            qe_s[pl.ds(at[u], PAIR), :] = qe.astype(BF16)
            work.append((qs.astype(BF16), ks.astype(BF16), ke.astype(BF16), jnp.exp(end0), jnp.exp(end1)))
        scores = [lax.dot_general(w[1], w[0], NT, preferred_element_type=F32) for w in work]
        updates = []
        for u in range(U1):
            vt = v_s[:, pl.ds(at[u], PAIR)]
            both = jnp.where(maskt, scores[u], 0.0).astype(BF16)
            yw_s[:, pl.ds(at[u], PAIR)] = jnp.dot(vt, both, preferred_element_type=F32)
            zero = jnp.zeros_like(vt)
            split = jnp.concatenate([jnp.where(left, vt, zero), jnp.where(left, zero, vt)], axis=0)
            updates.append(jnp.dot(split, work[u][2], preferred_element_type=F32))
        for u in range(U1):
            d0, d1 = work[u][3], work[u][4]
            middle = d0 * state + updates[u][0:BLOCK, :]
            pre_s[pl.ds(at[u], BLOCK), :] = state
            pre_s[pl.ds(pl.multiple_of(at[u] + BLOCK, BLOCK), BLOCK), :] = middle
            half = decay * d0
            dec_s[pl.ds(pl.multiple_of((i * U1 + u) * 8, 8), 8), :] = jnp.concatenate(
                [decay, half, jnp.zeros((6, KEY_DIM), F32)], axis=0
            )
            state = d1 * middle + updates[u][BLOCK:PAIR, :]
            decay = half * d1
        return state, decay

    state, decay = lax.fori_loop(
        0, TOK // (PAIR * U1), local_pairs,
        (jnp.zeros((VAL_DIM, KEY_DIM), F32), jnp.ones((1, KEY_DIM), F32)),
    )
    decay_hi = decay.astype(BF16).astype(F32)
    row16 = lax.broadcasted_iota(jnp.int32, (16, KEY_DIM), 0)
    tail = jnp.where(row16 == 0, decay_hi, jnp.where(row16 == 1, decay - decay_hi, 0.0))
    cs_s[0:VAL_DIM, :] = state.astype(BF16)
    cs_s[VAL_DIM : VAL_DIM + 16, :] = tail.astype(BF16)
    cr_s[me] = jnp.zeros((VAL_DIM + 16, KEY_DIM), BF16)

    def hand_on(k):
        return remote(cs_s, cr_s.at[me], csend.at[k], crecv.at[me], moved(me, offs[k], E), t)

    def handed(k):
        source = moved(me, offs[k], E, back=True)
        return remote(cs_s, cr_s.at[source], csend.at[k], crecv.at[source], source, t)

    for k in range(1, E):
        hand_on(k).start()
    for g in range(1, NG):
        fill_group(g)
        for k in range(g * KG, (g + 1) * KG):
            dispatch(k).start()

    for k in range(1, E):
        handed(k).wait_recv()
    start = jnp.zeros((VAL_DIM, KEY_DIM), F32)
    for j in range(E - 1):
        ends = cr_s[j, VAL_DIM : VAL_DIM + 16, :].astype(F32)
        after = (ends[0:1, :] + ends[1:2, :]) * start + cr_s[j, 0:VAL_DIM, :].astype(F32)
        start = jnp.where(j < me, after, start)
    ga = lax.broadcasted_iota(jnp.int32, (VAL_DIM, VAL_DIM), 0)
    gb = lax.broadcasted_iota(jnp.int32, (VAL_DIM, VAL_DIM), 1)
    head_gain = jnp.sum(jnp.where(ga == gb, hgain_ref[...], 0.0), axis=-1, keepdims=True)
    own_rows = pl.multiple_of(t * VAL_DIM, VAL_DIM)

    def finish_pairs(i, carry):
        left = lax.broadcasted_iota(jnp.int32, (BLOCK, PAIR), 1) < BLOCK
        at = [pl.multiple_of((i * U1 + u) * PAIR, PAIR) for u in range(U1)]
        across = []
        for u in range(U1):
            d = dec_s[pl.ds(pl.multiple_of((i * U1 + u) * 8, 8), 8), :]
            s0 = pre_s[pl.ds(at[u], BLOCK), :] + d[0:1, :] * start
            s1 = pre_s[pl.ds(pl.multiple_of(at[u] + BLOCK, BLOCK), BLOCK), :] + d[1:2, :] * start
            states = jnp.concatenate([s0, s1], axis=0).astype(BF16)
            across.append(
                lax.dot_general(states, qe_s[pl.ds(at[u], PAIR), :], NT, preferred_element_type=F32)
            )
        for u in range(U1):
            cols = pl.ds(at[u], PAIR)
            y = yw_s[:, cols] + jnp.where(left, across[u][0:BLOCK, :], across[u][BLOCK:PAIR, :])
            factor = lax.rsqrt(jnp.mean(y * y, axis=0, keepdims=True) + EPS)
            gate = o_s[:, cols].astype(F32)
            gate = gate * (1.0 / (1.0 + jnp.exp(-gate)))
            m_s[pl.ds(own_rows, VAL_DIM), cols] = (y * factor * head_gain * gate).astype(BF16)
        return carry

    lax.fori_loop(0, TOK // (PAIR * U1), finish_pairs, 0)

    VH = VAL_DIM // 2
    reach = {(1, 0): Z // 2, (1, 1): Z - 1 - Z // 2, (-1, 0): Z - 1 - Z // 2, (-1, 1): Z // 2}

    def head_at(zz, core):
        return pl.multiple_of((lax.rem(zz + 2 * Z, Z) * 2 + core) * VAL_DIM, VAL_DIM)

    def ring(way, half, hop):
        rows = pl.ds(pl.multiple_of(head_at(z - way * (hop - 1), c) + half * VH, VH), VH)
        w = 0 if way == 1 else 1
        return remote(
            m_s.at[rows, :], m_s.at[rows, :], msend.at[w, half, hop - 1], mrecv.at[w, half, hop - 1],
            me, lax.rem(z + way + Z, Z) * 2 + c,
        )

    def ringed(way, half, hop):
        rows = pl.ds(pl.multiple_of(head_at(z - way * hop, c) + half * VH, VH), VH)
        w = 0 if way == 1 else 1
        return remote(
            m_s.at[rows, :], m_s.at[rows, :], msend.at[w, half, hop - 1], mrecv.at[w, half, hop - 1],
            me, lax.rem(z + way + Z, Z) * 2 + c,
        )

    def share(r, core):
        rows = pl.ds(head_at(z - r, core), VAL_DIM)
        return remote(m_s.at[rows, :], m_s.at[rows, :], dsend.at[r], drecv.at[r], me, z * 2 + pc)

    lanes = [(1, 0), (-1, 1), (1, 1), (-1, 0)]

    def relay(hop):
        for way, half in lanes:
            if hop <= reach[way, half]:
                ringed(way, half, hop).wait_recv()
                if hop + 1 <= reach[way, half]:
                    ring(way, half, hop + 1).start()
        if hop == Z - hop:
            share(hop, c).start()
        elif hop < Z - hop:
            share(hop, c).start()
            share(Z - hop, c).start()

    for way, half in lanes:
        if reach[way, half] >= 1:
            ring(way, half, 1).start()
    share(0, c).start()

    def forward_group(g):
        for k in range(g * KG, (g + 1) * KG):
            if k:
                dispatch(k).wait_recv()
            forward(k).start()

    def ffn(g):
        rows = slice(g * GR, (g + 1) * GR)
        for k in range(g * KG, (g + 1) * KG):
            back = slice(k * KR, (k + 1) * KR)
            remote(
                r_s.at[c, back, :], r_s.at[pc, back, :], fsend.at[k], frecv.at[k], me, z * 2 + pc
            ).wait_recv()
        a, b = r_s[0, rows, :], r_s[1, rows, :]
        gate = lax.dot_general(a, wg_s[:, 0:H], NT, preferred_element_type=F32) + lax.dot_general(
            b, wg_s[:, H:D], NT, preferred_element_type=F32
        )
        up = lax.dot_general(a, wu_s[:, 0:H], NT, preferred_element_type=F32) + lax.dot_general(
            b, wu_s[:, H:D], NT, preferred_element_type=F32
        )
        hid_s[...] = (gate * (1.0 / (1.0 + jnp.exp(-gate))) * up).astype(BF16)
        hid = hid_s[...]
        for zz in range(Z):
            y = jnp.dot(hid, wd_s[:, zz * 256 : zz * 256 + 256], preferred_element_type=F32).astype(BF16)
            pp_s[0, zz, rows, :] = y[:, 0:128]
            pp_s[1, zz, rows, :] = y[:, 128:256]
        swap(g).start()

    def swap(g):
        rows = slice(g * GR, (g + 1) * GR)
        return remote(
            pp_s.at[pc, :, rows, :], qb_s.at[:, rows, :], psend.at[g], precv.at[g], me, z * 2 + pc
        )

    def way_of(g):
        return 1 if g % 2 == 0 else -1

    def pass_on(g, s):
        way = way_of(g)
        rows = slice(g * GR, (g + 1) * GR)
        part = lax.rem(z - way * (1 + s) + 2 * Z, Z)
        return remote(
            pp_s.at[c, part, rows, :], rb_s.at[s, rows, :], bsend.at[s, g], brecv.at[s, g],
            me, lax.rem(z + way + Z, Z) * 2 + c,
        )

    def add_and_pass(g, s):
        way = way_of(g)
        rows = slice(g * GR, (g + 1) * GR)
        part = lax.rem(z - way * (1 + s) + 2 * Z, Z)
        total = pp_s[c, part, rows, :].astype(F32) + qb_s[part, rows, :].astype(F32)
        if s:
            pass_on(g, s - 1).wait_recv()
            total = total + rb_s[s - 1, rows, :].astype(F32)
        if s < Z - 1:
            pp_s[c, part, rows, :] = total.astype(BF16)
            pass_on(g, s).start()
        else:
            fs_s[rows, :] = total.astype(BF16)

    forward_group(0)
    order = [("relay", 1), ("ffn", 0)]
    hops = max(reach.values())
    for g in range(1, NG):
        order += [("forward", g)]
        if g + 1 <= hops:
            order += [("relay", g + 1)]
        order += [("ffn", g)]
    for hop in range(NG + 1, hops + 1):
        order += [("relay", hop)]
    for load in loads[6:]:
        load.wait()
    for what, n in order:
        if what == "relay":
            relay(n)
        elif what == "forward":
            forward_group(n)
        else:
            ffn(n)
    for g in range(NG):
        swap(g).wait_recv()
        add_and_pass(g, 0)

    def project(n):
        for r in range(Z) if n == 0 else ():
            share(r, pc).wait_recv()
        cols = slice(n * (TOK // 4), (n + 1) * (TOK // 4))
        outt = lax.dot_general(
            wo_s[...], m_s[:, cols], (((0,), (0,)), ((), ())), preferred_element_type=F32
        )
        out_s[cols, :] = outt.T.astype(BF16)

    def weigh(g):
        for k in range(g * KG, (g + 1) * KG):
            rows = slice(k * KR, (k + 1) * KR)
            gh_s[rows, :] = g_s[rows, :] * weight_hi[k : k + 1, :]
            gl_s[rows, :] = g_s[rows, :] * weight_lo[k : k + 1, :]

    side = [functools.partial(project, n) for n in range(4)] + [functools.partial(weigh, g) for g in range(NG)]
    out_copy = pltpu.make_async_copy(out_s, out_hbm, osem)
    for s in range(1, Z):
        for g in range(NG):
            add_and_pass(g, s)
        if s < Z - 1:
            for _ in range(-(-len(side) // max(1, Z - 1 - s))):
                side.pop(0)()
    out_copy.start()

    def give_back(k):
        rows = slice(k * KR, (k + 1) * KR)
        return remote(
            fs_s.at[rows, :], rr_s.at[rows, :], rsend.at[k], rrecv.at[k], moved(me, offs[k], E, back=True), t
        )

    for k in range(1, E):
        give_back(k).start()
    rr_s[0:KR, :] = fs_s[0:KR, :]
    for k in range(1, E):
        give_back(k).wait_recv()
    results = rr_s[...].T
    combined = jnp.dot(results, gh_s[...], preferred_element_type=F32) + jnp.dot(
        results, gl_s[...], preferred_element_type=F32
    )
    co_s[...] = combined.T.astype(BF16)

    def scatter(j):
        to = lax.rem(t + j, TP)
        return remote(
            co_s.at[pl.ds(pl.multiple_of(to * SUB, SUB), SUB), :], fo_s.at[t], zsend.at[j], zrecv.at[j], me, to
        )

    for j in range(1, TP):
        scatter(j).start()
    fo_s[t] = co_s[pl.ds(pl.multiple_of(t * SUB, SUB), SUB), :]
    for j in range(1, TP):
        source = lax.rem(t + TP - j, TP)
        remote(co_s.at[0:SUB, :], fo_s.at[source], zsend.at[j], zrecv.at[j], me, source).wait_recv()
    for j in range(TP):
        moe_ref[:, j * 128 : (j + 1) * 128] = fo_s[j]

    for k in range(1, E):
        dispatch(k).wait_send()
        hand_on(k).wait_send()
        give_back(k).wait_send()
    for k in range(E):
        forward(k).wait_send()
    for way, half in lanes:
        for hop in range(1, reach[way, half] + 1):
            ring(way, half, hop).wait_send()
    for r in range(Z):
        share(r, c).wait_send()
    for g in range(NG):
        swap(g).wait_send()
        for s in range(Z - 1):
            pass_on(g, s).wait_send()
    for j in range(1, TP):
        scatter(j).wait_send()
    out_copy.wait()


def on_device(
    query, forget, values, out_gate, gap, extra, head_gain, w_out,
    tokens, ff_gain, chosen, chosen_w, w_gate, w_up, w_down,
):
    E, TP = w_gate.shape[0] * lax.axis_size("ep"), lax.axis_size("tp")
    TOK, D = query.shape[0], tokens.shape[1]
    NTOK, FF = tokens.shape[0], w_gate.shape[2]
    SUB = NTOK // TP
    CAP = max(2, SUB * TOPK * 5 // (4 * E))
    Z, KR = TP // 2, TP * CAP
    ROWS, H = E * KR, D // 2
    KG = max(1, E // 4)
    NG = E // KG
    cfg = dict(E=E, TP=TP, TOK=TOK, SUB=SUB, CAP=CAP)
    any_spec = pl.BlockSpec(memory_space=pl.ANY)
    vmem = pl.BlockSpec(memory_space=pltpu.VMEM)
    dma = pltpu.SemaphoreType.DMA
    V = pltpu.VMEM
    hops = Z // 2
    return pl.pallas_call(
        functools.partial(kernel, cfg),
        out_shape=(
            jax.ShapeDtypeStruct((TOK, w_out.shape[1]), BF16),
            jax.ShapeDtypeStruct((SUB, D), BF16),
        ),
        in_specs=[any_spec] * 4 + [vmem] * 3 + [any_spec] * 2 + [vmem] * 3 + [any_spec] * 3,
        out_specs=(any_spec, vmem),
        scratch_shapes=[
            V((TOK, KEY_DIM), BF16), V((TOK, KEY_DIM), BF16), V((VAL_DIM, TOK), BF16), V((VAL_DIM, TOK), BF16),
            V(w_out.shape, BF16), V((2, NTOK, H), BF16), V((FF, D), BF16), V((FF, D), BF16), V((FF, D), BF16),
            V((PAIR, PAIR), F32), V((TOK // PAIR * 8, KEY_DIM), F32), V((TOK, KEY_DIM), F32),
            V((VAL_DIM, TOK), F32), V((TOK, KEY_DIM), BF16), V((VAL_DIM + 16, KEY_DIM), BF16),
            V((E, VAL_DIM + 16, KEY_DIM), BF16),
            V((NTOK, H), BF16), V((E, NTOK), F32), V((ROWS, NTOK), BF16), V((ROWS, H), BF16),
            V((2, ROWS, H), BF16), V((KG * KR, FF), BF16), V((2, Z, ROWS, 128), BF16),
            V((Z, ROWS, 128), BF16), V((Z - 1, ROWS, 128), BF16),
            V((TP * VAL_DIM, TOK), BF16), V((TOK, w_out.shape[1]), BF16), V((ROWS, 128), BF16),
            V((ROWS, 128), BF16), V((ROWS, NTOK), BF16), V((ROWS, NTOK), BF16), V((NTOK, 128), BF16),
            V((TP, SUB, 128), BF16),
            dma((10,)), dma, dma((E,)), dma((E,)), dma((E,)), dma((E,)), dma((E,)), dma((E,)),
            dma((2, 2, hops)), dma((2, 2, hops)), dma((Z,)), dma((Z,)), dma((NG,)), dma((NG,)),
            dma((Z - 1, NG)), dma((Z - 1, NG)), dma((E,)), dma((E,)), dma((TP,)), dma((TP,)),
        ],
        compiler_params=pltpu.CompilerParams(
            collective_id=0, has_side_effects=True, vmem_limit_bytes=64000 * 1024
        ),
    )(
        query, forget, values.T, out_gate.T, gap.reshape(1, -1), extra.T, head_gain.reshape(1, -1), w_out,
        tokens, ff_gain.reshape(1, -1), chosen.T, chosen_w.T, w_gate[0].T, w_up[0].T, w_down[0],
    )


def solution(mesh):
    placed = (
        P("ep", "tp"), P("ep", "tp"), P("ep", "tp"), P("ep", "tp"), P("tp"), P("ep", "tp"), P("tp"),
        P(None, "tp"), P("ep", None), P(), P("ep", None), P("ep", None),
        P("ep", None, "tp"), P("ep", None, "tp"), P("ep", "tp", None),
    )
    return jax.shard_map(
        on_device,
        mesh=mesh,
        in_specs=placed,
        out_specs=(P("ep", "tp"), P(("ep", "tp"), None)),
        check_vma=False,
    )
```

time: 236 us -> 111 us (0.47)
  Pallas kernels: 0 us -> 107 us
  waiting for transfers between devices: 96.6 us -> 0 us
  local copies, waits for them, and re-layouts: 53.1 us -> 3.44 us
  matrix products: 25.2 us -> 0 us
  blocking collectives: 17.8 us -> 0 us
  other arithmetic: 14.4 us -> 0 us
  between operations: 14.5 us -> 0.65 us
  starting transfers between devices: 13 us -> 0 us
    pallas_call x0 -> x1, Pallas kernels: none -> 107 us  [on_device(): pl.pallas_call(functools.partial(kernel, cfg), out_shape=(jax.ShapeDtypeS...]
    all_gather x2 -> x0, waiting for transfers between devices: 80.5 us -> none  [the longest x1 42.5 us: on_device(): segment = lax.all_gather(arrived[None], 'tp', axis=0, tiled=True)]
    dot_general x6 -> x0, matrix products: 25.2 us -> none  [the longest x1 10.4 us: on_device(): jnp.einsum('tsecf,efd->tsecd', hidden, expert_down_weight, preferred_elem...]
    convert_element_type x6 -> x0, local copies, waits for them, and re-layouts: 20.6 us -> none  [the longest x2 20.4 us: on_device(): product.reshape(rows_each * lax.axis_size('tp'), product.shape[-1])]
    all_to_all x1 -> x0, blocking collectives: 17.8 us -> none  [on_device(): lax.all_to_all(outgoing, 'ep', split_axis=0, concat_axis=0, tiled=True)]
    reduce_scatter x1 -> x0, waiting for transfers between devices: 16 us -> none  [on_device(): lax.psum_scatter(product.reshape(rows_each * lax.axis_size('tp'), product...]
    all_to_all x2 -> x0, starting transfers between devices: 12.9 us -> none  [the longest x1 6.58 us: copy_for_each(): return lax.all_to_all(copies, axis, split_axis=0, concat_axis=0, tiled=True)]
    pad x16 -> x0, local copies, waits for them, and re-layouts: 12.7 us -> none  [on_device(): lax.associative_scan(combine_states, (decays, updates))]
  transfers between devices with their start and end apart: 5 -> 0, of which waited for: 3 -> 0; matrix products, arithmetic and copies ran while one was open for 19% -> 0% of each run, Pallas kernels for 0% -> 0%
where the time goes in v1:
time: 111 us
  Pallas kernels  107 us (96%)
  local copies, waits for them, and re-layouts  3.44 us (3%)
    pallas_call x1, Pallas kernels, on_device(): pl.pallas_call(functools.partial(kernel, cfg), out_shape=(jax.ShapeDtypeS...  107 us
    unnamed x2, local copies, waits for them, and re-layouts  3.44 us

profile of v1, /device:TPU:1, one launch (start us, length us, event | category | flops | bytes accessed | tf_op | source)
XLA Modules:
  0.0 111.2 jit_solution(14254887118415588765)
XLA Ops:
  0.6 107.2 %shard_map.158 = (bf16[2048,128]{1,0:T(8,128)(2,1)}, bf16[32,2048]{1,0:T(8,128)(2,1)}) custom-call(bf16[2048,128]{1,0:T(8,128)(2,1)} %q_hbm.1, bf16[2048,128]{1,0:T(8,128)(2,1)} %f_hbm.1, bf16[64,2048]{1,0:T(8,128)(2,1)} %bitcast.18, bf16[64,2048]{1,0:T(8,128)(2,1)} %bitcast.19, f32[1,128]{1,0:T(1,128)} %bitcast.24, f32[1,2048]{1,0:T(1,128)} %bitcast.20, ...), custom_call_target="tpu_custom_call" | custom-call | tf_op jit(solution)/shard_map/pallas_call | solution.py:503
  107.8 1.9 %copy.19 = bf16[2048,128]{1,0:T(8,128)(2,1)} copy(bf16[2048,128]{1,0:T(8,128)(2,1)} %get-tuple-element.4) | data formatting | bytes 1048576
  109.7 1.6 %copy.20 = bf16[32,2048]{1,0:T(8,128)(2,1)} copy(bf16[32,2048]{1,0:T(8,128)(2,1)} %get-tuple-element.5) | data formatting | bytes 262144

commit v2 on v1

--- a/solution.py
+++ b/solution.py
@@ -22,10 +22,10 @@
 def offsets(experts):
     if experts == 16:
         return [
-            (0, 0), (0, 1), (3, 0), (0, 3),
-            (1, 0), (1, 1), (3, 3), (1, 3),
-            (3, 1), (0, 2), (2, 0), (1, 2),
-            (2, 3), (3, 2), (2, 1), (2, 2),
+            (0, 0), (2, 2), (1, 2), (2, 1),
+            (3, 2), (2, 3), (0, 2), (2, 0),
+            (1, 1), (3, 3), (1, 3), (3, 1),
+            (0, 1), (3, 0), (0, 3), (1, 0),
         ]
     return [(0, k) for k in range(experts)]
 
@@ -47,8 +47,8 @@
     out_hbm, moe_ref,
     q_s, f_s, v_s, o_s, wo_s, x_s, wg_s, wu_s, wd_s,
     tri_s, dec_s, pre_s, yw_s, qe_s, cs_s, cr_s,
-    n_s, slot_s, g_s, s_s, r_s, hid_s, pp_s, qb_s, rb_s,
-    m_s, out_s, fs_s, rr_s, gh_s, gl_s, co_s, fo_s,
+    n_s, slot_s, g_s, s_s, r_s, hid_s, hp_s, pp_s, qb_s, rb_s,
+    perm_s, perm_back_s, m_s, out_s, fs_s, fb_s, rr_s, gh_s, gl_s, co_s, mo_s,
     lsem, osem, asend, arecv, fsend, frecv, csend, crecv,
     msend, mrecv, dsend, drecv, psend, precv, bsend, brecv, rsend, rrecv, zsend, zrecv,
 ):
@@ -58,8 +58,14 @@
     KG = max(1, E // 4)
     NG = E // KG
     GR = KG * KR
+    UNIT = 2 * CAP
+    SG = max(1, E // 2)
+    NS = E // SG
+    SR = SG * UNIT
     D = x_hbm.shape[1]
     H = D // 2
+    W = H // 2
+    J = H // 128
     NTOK = x_hbm.shape[0]
     offs = offsets(E)
     me = lax.axis_index("ep")
@@ -83,8 +89,8 @@
     barrier = pltpu.get_barrier_semaphore()
     for k in range(1, E):
         pl.semaphore_signal(barrier, inc=1, device_id=(moved(me, offs[k], E), t), device_id_type=MESH)
-    for j in range(1, TP):
-        pl.semaphore_signal(barrier, inc=1, device_id=(me, lax.rem(t + j, TP)), device_id_type=MESH)
+    for j in (z * 2 + pc, lax.rem(z + 1, Z) * 2 + c, lax.rem(z + Z - 1, Z) * 2 + c):
+        pl.semaphore_signal(barrier, inc=1, device_id=(me, j), device_id_type=MESH)
 
     i0, i1 = idx_ref[0:1, :], idx_ref[1:2, :]
     row_e = lax.broadcasted_iota(jnp.int32, (E, NTOK), 0)
@@ -144,9 +150,6 @@
 
     fill_group(0)
     r_s[c, 0:KR, :] = s_s[0:KR, :]
-    pl.semaphore_wait(barrier, E - 1 + TP - 1)
-    for k in range(1, KG):
-        dispatch(k).start()
 
     ta = lax.broadcasted_iota(jnp.int32, (PAIR, PAIR), 0)
     tb = lax.broadcasted_iota(jnp.int32, (PAIR, PAIR), 1)
@@ -234,12 +237,24 @@
         source = moved(me, offs[k], E, back=True)
         return remote(cs_s, cr_s.at[source], csend.at[k], crecv.at[source], source, t)
 
+    pl.semaphore_wait(barrier, E - 1 + 3)
     for k in range(1, E):
         hand_on(k).start()
+    for k in range(1, KG):
+        dispatch(k).start()
     for g in range(1, NG):
         fill_group(g)
         for k in range(g * KG, (g + 1) * KG):
             dispatch(k).start()
+
+    def swapper(ref, outer, inner):
+        size = outer * inner * UNIT
+        row = lax.broadcasted_iota(jnp.int32, (size, 1), 0)
+        source = (row // UNIT % inner * outer + row // (inner * UNIT)) * UNIT + row % UNIT
+        ref[...] = jnp.where(lax.broadcasted_iota(jnp.int32, (size, size), 1) == source, 1.0, 0.0).astype(BF16)
+
+    swapper(perm_s, Z, SG)
+    swapper(perm_back_s, SG, J)
 
     for k in range(1, E):
         handed(k).wait_recv()
@@ -341,68 +356,91 @@
         up = lax.dot_general(a, wu_s[:, 0:H], NT, preferred_element_type=F32) + lax.dot_general(
             b, wu_s[:, H:D], NT, preferred_element_type=F32
         )
-        hid_s[...] = (gate * (1.0 / (1.0 + jnp.exp(-gate))) * up).astype(BF16)
-        hid = hid_s[...]
-        for zz in range(Z):
-            y = jnp.dot(hid, wd_s[:, zz * 256 : zz * 256 + 256], preferred_element_type=F32).astype(BF16)
-            pp_s[0, zz, rows, :] = y[:, 0:128]
-            pp_s[1, zz, rows, :] = y[:, 128:256]
-        swap(g).start()
-
-    def swap(g):
-        rows = slice(g * GR, (g + 1) * GR)
+        hid_s[rows, :] = (gate * (1.0 / (1.0 + jnp.exp(-gate))) * up).astype(BF16)
+
+    def relative(r):
+        return lax.rem(z + r + 2 * Z, Z)
+
+    def swap(g, r):
+        part = relative(r)
         return remote(
-            pp_s.at[pc, :, rows, :], qb_s.at[:, rows, :], psend.at[g], precv.at[g], me, z * 2 + pc
-        )
-
-    def way_of(g):
-        return 1 if g % 2 == 0 else -1
-
-    def pass_on(g, s):
-        way = way_of(g)
-        rows = slice(g * GR, (g + 1) * GR)
-        part = lax.rem(z - way * (1 + s) + 2 * Z, Z)
+            pp_s.at[pc, :, g, part], qb_s.at[:, g, part], psend.at[g, r % Z], precv.at[g, r % Z],
+            me, z * 2 + pc,
+        )
+
+    def pass_on(g, d, s):
+        way = 1 - 2 * d
+        part = relative(-way * (1 + s))
         return remote(
-            pp_s.at[c, part, rows, :], rb_s.at[s, rows, :], bsend.at[s, g], brecv.at[s, g],
-            me, lax.rem(z + way + Z, Z) * 2 + c,
-        )
-
-    def add_and_pass(g, s):
-        way = way_of(g)
-        rows = slice(g * GR, (g + 1) * GR)
-        part = lax.rem(z - way * (1 + s) + 2 * Z, Z)
-        total = pp_s[c, part, rows, :].astype(F32) + qb_s[part, rows, :].astype(F32)
+            pp_s.at[c, d, g, part], rb_s.at[s, g, d], bsend.at[s, g, d], brecv.at[s, g, d],
+            me, relative(way) * 2 + c,
+        )
+
+    swapped = set()
+
+    def add_and_pass(g, d, s):
+        r = -(1 - 2 * d) * (1 + s)
+        part = relative(r)
+        if (g, r % Z) not in swapped:
+            swapped.add((g, r % Z))
+            swap(g, r).wait_recv()
+        total = pp_s[c, d, g, part].astype(F32) + qb_s[d, g, part].astype(F32)
         if s:
-            pass_on(g, s - 1).wait_recv()
-            total = total + rb_s[s - 1, rows, :].astype(F32)
+            pass_on(g, d, s - 1).wait_recv()
+            total = total + rb_s[s - 1, g, d].astype(F32)
         if s < Z - 1:
-            pp_s[c, part, rows, :] = total.astype(BF16)
-            pass_on(g, s).start()
+            pp_s[c, d, g, part] = total.astype(BF16)
+            pass_on(g, d, s).start()
         else:
-            fs_s[rows, :] = total.astype(BF16)
-
-    forward_group(0)
-    order = [("relay", 1), ("ffn", 0)]
+            for n in range(W // 128):
+                at = (d * (W // 128) + n) * SR
+                fs_s[g, at : at + SR, :] = total[:, n * 128 : n * 128 + 128].astype(BF16)
+
+    def down(g):
+        rows = slice(g * Z * SR, (g + 1) * Z * SR)
+        hp_s[rows, :] = jnp.dot(
+            perm_s[...], hid_s[rows, :], preferred_element_type=F32
+        ).astype(BF16)
+        turns = [r for n in range(1, Z // 2) for r in (-n, n)] + [Z // 2, 0]
+        for n in range(0, Z, 2):
+            pair = turns[n : n + 2]
+            hid = jnp.concatenate(
+                [
+                    hp_s[pl.ds(pl.multiple_of((g * Z + relative(r)) * SR, 16), SR), :]
+                    for r in pair
+                ],
+                axis=0,
+            )
+            for half in range(2):
+                for d in range(2):
+                    cols = slice(half * H + d * W, half * H + (d + 1) * W)
+                    y = jnp.dot(hid, wd_s[:, cols], preferred_element_type=F32).astype(BF16)
+                    for i, r in enumerate(pair):
+                        pp_s[half, d, g, relative(r)] = y[i * SR : (i + 1) * SR, :]
+            for r in pair:
+                swap(g, r).start()
+            if n == min(2, Z - 2):
+                for d in range(2):
+                    add_and_pass(g, d, 0)
+
     hops = max(reach.values())
-    for g in range(1, NG):
-        order += [("forward", g)]
-        if g + 1 <= hops:
-            order += [("relay", g + 1)]
-        order += [("ffn", g)]
-    for hop in range(NG + 1, hops + 1):
-        order += [("relay", hop)]
     for load in loads[6:]:
         load.wait()
-    for what, n in order:
-        if what == "relay":
-            relay(n)
-        elif what == "forward":
-            forward_group(n)
-        else:
-            ffn(n)
+    forward_group(0)
+    done = 0
     for g in range(NG):
-        swap(g).wait_recv()
-        add_and_pass(g, 0)
+        ffn(g)
+        if g + 1 < NG:
+            forward_group(g + 1)
+        if g + 1 <= hops:
+            relay(g + 1)
+        while done < NS and (done + 1) * SG <= (g + 1) * KG:
+            down(done)
+            done += 1
+    for hop in range(NG + 1, hops + 1):
+        relay(hop)
+
+    out_copy = pltpu.make_async_copy(out_s, out_hbm, osem)
 
     def project(n):
         for r in range(Z) if n == 0 else ():
@@ -412,54 +450,77 @@
             wo_s[...], m_s[:, cols], (((0,), (0,)), ((), ())), preferred_element_type=F32
         )
         out_s[cols, :] = outt.T.astype(BF16)
-
-    def weigh(g):
-        for k in range(g * KG, (g + 1) * KG):
-            rows = slice(k * KR, (k + 1) * KR)
-            gh_s[rows, :] = g_s[rows, :] * weight_hi[k : k + 1, :]
-            gl_s[rows, :] = g_s[rows, :] * weight_lo[k : k + 1, :]
-
-    side = [functools.partial(project, n) for n in range(4)] + [functools.partial(weigh, g) for g in range(NG)]
-    out_copy = pltpu.make_async_copy(out_s, out_hbm, osem)
+        if n == 3:
+            out_copy.start()
+
+    lanes_out = J * 2 * SUB
+    lane = lax.broadcasted_iota(jnp.int32, (1, lanes_out), 1)
+
+    def weigh_all():
+        token = lax.broadcasted_iota(jnp.int32, (NTOK, lanes_out), 0)
+        mine = z * 2 * SUB + lane % (2 * SUB)
+        pick = jnp.where(token == mine, 1.0, 0.0).astype(BF16)
+        local = slot_s[...] - (z * UNIT).astype(F32)
+        local = jnp.where((local >= 0) & (local < UNIT), local, -1.0).astype(BF16)
+        place_at = jnp.dot(local, pick, preferred_element_type=F32)
+        high = jnp.dot(weight_hi, pick, preferred_element_type=F32)
+        low = jnp.dot(weight_lo, pick, preferred_element_type=F32)
+        shift = (lane // (2 * SUB) * UNIT).astype(F32)
+        target = jnp.where(place_at >= 0, place_at + shift, -1.0)
+        row = lax.broadcasted_iota(jnp.int32, (J * UNIT, lanes_out), 0).astype(F32)
+        for k in range(E):
+            rows = slice(k * J * UNIT, (k + 1) * J * UNIT)
+            here = row == target[k : k + 1, :]
+            gh_s[rows, :] = jnp.where(here, high[k : k + 1, :], 0.0).astype(BF16)
+            gl_s[rows, :] = jnp.where(here, low[k : k + 1, :], 0.0).astype(BF16)
+
+    BR = J * UNIT
+
+    def give_back(k):
+        rows = slice(k * BR, (k + 1) * BR)
+        return remote(
+            fb_s.at[rows, :], rr_s.at[rows, :], rsend.at[k], rrecv.at[k], moved(me, offs[k], E, back=True), t
+        )
+
+    side = [functools.partial(project, n) for n in range(4)] + [weigh_all]
     for s in range(1, Z):
-        for g in range(NG):
-            add_and_pass(g, s)
+        for g in range(NS):
+            for d in range(2):
+                add_and_pass(g, d, s)
+            if s == Z - 1:
+                rows = slice(g * SG * BR, (g + 1) * SG * BR)
+                fb_s[rows, :] = jnp.dot(
+                    perm_back_s[...], fs_s[g], preferred_element_type=F32
+                ).astype(BF16)
+                for k in range(g * SG, (g + 1) * SG):
+                    if k:
+                        give_back(k).start()
         if s < Z - 1:
             for _ in range(-(-len(side) // max(1, Z - 1 - s))):
                 side.pop(0)()
-    out_copy.start()
-
-    def give_back(k):
-        rows = slice(k * KR, (k + 1) * KR)
-        return remote(
-            fs_s.at[rows, :], rr_s.at[rows, :], rsend.at[k], rrecv.at[k], moved(me, offs[k], E, back=True), t
-        )
-
-    for k in range(1, E):
-        give_back(k).start()
-    rr_s[0:KR, :] = fs_s[0:KR, :]
+    while side:
+        side.pop(0)()
+    rr_s[0:BR, :] = fb_s[0:BR, :]
     for k in range(1, E):
         give_back(k).wait_recv()
     results = rr_s[...].T
     combined = jnp.dot(results, gh_s[...], preferred_element_type=F32) + jnp.dot(
         results, gl_s[...], preferred_element_type=F32
     )
-    co_s[...] = combined.T.astype(BF16)
-
-    def scatter(j):
-        to = lax.rem(t + j, TP)
-        return remote(
-            co_s.at[pl.ds(pl.multiple_of(to * SUB, SUB), SUB), :], fo_s.at[t], zsend.at[j], zrecv.at[j], me, to
-        )
-
-    for j in range(1, TP):
-        scatter(j).start()
-    fo_s[t] = co_s[pl.ds(pl.multiple_of(t * SUB, SUB), SUB), :]
-    for j in range(1, TP):
-        source = lax.rem(t + TP - j, TP)
-        remote(co_s.at[0:SUB, :], fo_s.at[source], zsend.at[j], zrecv.at[j], me, source).wait_recv()
-    for j in range(TP):
-        moe_ref[:, j * 128 : (j + 1) * 128] = fo_s[j]
+    combined = combined.T.astype(BF16)
+    for j in range(J):
+        co_s[j] = combined[j * 2 * SUB : (j + 1) * 2 * SUB, :]
+
+    def hand_over(core):
+        mine = pl.ds(pl.multiple_of((1 - core) * SUB, SUB), SUB)
+        return remote(co_s.at[:, mine, :], mo_s.at[core], zsend, zrecv, me, z * 2 + pc)
+
+    hand_over(c).start()
+    mo_s[c] = co_s[:, pl.ds(pl.multiple_of(c * SUB, SUB), SUB), :]
+    hand_over(pc).wait_recv()
+    for half in range(2):
+        for j in range(J):
+            moe_ref[:, half * H + j * 128 : half * H + (j + 1) * 128] = mo_s[half, j]
 
     for k in range(1, E):
         dispatch(k).wait_send()
@@ -472,12 +533,13 @@
             ring(way, half, hop).wait_send()
     for r in range(Z):
         share(r, c).wait_send()
-    for g in range(NG):
-        swap(g).wait_send()
-        for s in range(Z - 1):
-            pass_on(g, s).wait_send()
-    for j in range(1, TP):
-        scatter(j).wait_send()
+    for g in range(NS):
+        for r in range(Z):
+            swap(g, r).wait_send()
+        for d in range(2):
+            for s in range(Z - 1):
+                pass_on(g, d, s).wait_send()
+    hand_over(c).wait_send()
     out_copy.wait()
 
 
@@ -494,6 +556,9 @@
     ROWS, H = E * KR, D // 2
     KG = max(1, E // 4)
     NG = E // KG
+    SG = max(1, E // 2)
+    NS, UNIT, J = E // SG, 2 * CAP, H // 128
+    SR = SG * UNIT
     cfg = dict(E=E, TP=TP, TOK=TOK, SUB=SUB, CAP=CAP)
     any_spec = pl.BlockSpec(memory_space=pl.ANY)
     vmem = pl.BlockSpec(memory_space=pltpu.VMEM)
@@ -515,14 +580,16 @@
             V((VAL_DIM, TOK), F32), V((TOK, KEY_DIM), BF16), V((VAL_DIM + 16, KEY_DIM), BF16),
             V((E, VAL_DIM + 16, KEY_DIM), BF16),
             V((NTOK, H), BF16), V((E, NTOK), F32), V((ROWS, NTOK), BF16), V((ROWS, H), BF16),
-            V((2, ROWS, H), BF16), V((KG * KR, FF), BF16), V((2, Z, ROWS, 128), BF16),
-            V((Z, ROWS, 128), BF16), V((Z - 1, ROWS, 128), BF16),
-            V((TP * VAL_DIM, TOK), BF16), V((TOK, w_out.shape[1]), BF16), V((ROWS, 128), BF16),
-            V((ROWS, 128), BF16), V((ROWS, NTOK), BF16), V((ROWS, NTOK), BF16), V((NTOK, 128), BF16),
-            V((TP, SUB, 128), BF16),
+            V((2, ROWS, H), BF16), V((ROWS, FF), BF16), V((ROWS, FF), BF16),
+            V((2, 2, NS, Z, SR, H // 2), BF16), V((2, NS, Z, SR, H // 2), BF16), V((Z - 1, NS, 2, SR, H // 2), BF16),
+            V((Z * SR, Z * SR), BF16), V((J * SR, J * SR), BF16),
+            V((TP * VAL_DIM, TOK), BF16), V((TOK, w_out.shape[1]), BF16), V((NS, J * SR, 128), BF16),
+            V((E * J * UNIT, 128), BF16), V((E * J * UNIT, 128), BF16),
+            V((E * J * UNIT, J * 2 * SUB), BF16), V((E * J * UNIT, J * 2 * SUB), BF16),
+            V((J, 2 * SUB, 128), BF16), V((2, J, SUB, 128), BF16),
             dma((10,)), dma, dma((E,)), dma((E,)), dma((E,)), dma((E,)), dma((E,)), dma((E,)),
-            dma((2, 2, hops)), dma((2, 2, hops)), dma((Z,)), dma((Z,)), dma((NG,)), dma((NG,)),
-            dma((Z - 1, NG)), dma((Z - 1, NG)), dma((E,)), dma((E,)), dma((TP,)), dma((TP,)),
+            dma((2, 2, hops)), dma((2, 2, hops)), dma((Z,)), dma((Z,)), dma((NS, Z)), dma((NS, Z)),
+            dma((Z - 1, NS, 2)), dma((Z - 1, NS, 2)), dma((E,)), dma((E,)), dma, dma,
         ],
         compiler_params=pltpu.CompilerParams(
             collective_id=0, has_side_effects=True, vmem_limit_bytes=64000 * 1024

time: 111 us -> 107 us (0.964)
  Pallas kernels: 107 us -> 103 us
    pallas_call x1, Pallas kernels: 107 us -> 103 us  [on_device(): pl.pallas_call(functools.partial(kernel, cfg), out_shape=(jax.ShapeDtypeS...]
where the time goes in v2:
time: 107 us
  Pallas kernels  103 us (96%)
  local copies, waits for them, and re-layouts  3.44 us (3%)
    pallas_call x1, Pallas kernels, on_device(): pl.pallas_call(functools.partial(kernel, cfg), out_shape=(jax.ShapeDtypeS...  103 us
    unnamed x2, local copies, waits for them, and re-layouts  3.44 us

profile of v2, /device:TPU:1, one launch (start us, length us, event | category | flops | bytes accessed | tf_op | source)
XLA Modules:
  0.0 106.8 jit_solution(16722319460736913484)
XLA Ops:
  0.6 102.8 %shard_map.158 = (bf16[2048,128]{1,0:T(8,128)(2,1)}, bf16[32,2048]{1,0:T(8,128)(2,1)}) custom-call(bf16[2048,128]{1,0:T(8,128)(2,1)} %q_hbm.1, bf16[2048,128]{1,0:T(8,128)(2,1)} %f_hbm.1, bf16[64,2048]{1,0:T(8,128)(2,1)} %bitcast.18, bf16[64,2048]{1,0:T(8,128)(2,1)} %bitcast.19, f32[1,128]{1,0:T(1,128)} %bitcast.24, f32[1,2048]{1,0:T(1,128)} %bitcast.20, ...), custom_call_target="tpu_custom_call" | custom-call | tf_op jit(solution)/shard_map/pallas_call | solution.py:568
  103.4 1.9 %copy.19 = bf16[2048,128]{1,0:T(8,128)(2,1)} copy(bf16[2048,128]{1,0:T(8,128)(2,1)} %get-tuple-element.4) | data formatting | bytes 1048576
  105.3 1.6 %copy.20 = bf16[32,2048]{1,0:T(8,128)(2,1)} copy(bf16[32,2048]{1,0:T(8,128)(2,1)} %get-tuple-element.5) | data formatting | bytes 262144

commit v3 on v2

--- a/solution.py
+++ b/solution.py
@@ -23,9 +23,9 @@
     if experts == 16:
         return [
             (0, 0), (2, 2), (1, 2), (2, 1),
-            (3, 2), (2, 3), (0, 2), (2, 0),
-            (1, 1), (3, 3), (1, 3), (3, 1),
-            (0, 1), (3, 0), (0, 3), (1, 0),
+            (3, 2), (2, 3), (0, 1), (3, 0),
+            (1, 1), (3, 3), (0, 2), (2, 0),
+            (1, 3), (3, 1), (0, 3), (1, 0),
         ]
     return [(0, k) for k in range(experts)]
 
@@ -47,7 +47,7 @@
     out_hbm, moe_ref,
     q_s, f_s, v_s, o_s, wo_s, x_s, wg_s, wu_s, wd_s,
     tri_s, dec_s, pre_s, yw_s, qe_s, cs_s, cr_s,
-    n_s, slot_s, g_s, s_s, r_s, hid_s, hp_s, pp_s, qb_s, rb_s,
+    n_s, slot_s, g_s, s_s, r_s, ga_s, ua_s, hid_s, hp_s, pp_s, qb_s, rb_s,
     perm_s, perm_back_s, m_s, out_s, fs_s, fb_s, rr_s, gh_s, gl_s, co_s, mo_s,
     lsem, osem, asend, arecv, fsend, frecv, csend, crecv,
     msend, mrecv, dsend, drecv, psend, precv, bsend, brecv, rsend, rrecv, zsend, zrecv,
@@ -64,7 +64,10 @@
     SR = SG * UNIT
     D = x_hbm.shape[1]
     H = D // 2
-    W = H // 2
+    ND = cfg["ND"]
+    W = H // ND
+    NW = cfg["NW"]
+    HW = H // NW
     J = H // 128
     NTOK = x_hbm.shape[0]
     offs = offsets(E)
@@ -79,8 +82,8 @@
         )
 
     loads = [
-        (x_hbm.at[:, 0:H], x_s.at[0]), (x_hbm.at[:, H:D], x_s.at[1]),
-        (f_hbm, f_s), (q_hbm, q_s), (v_hbm, v_s), (o_hbm, o_s),
+        (f_hbm, f_s), (q_hbm, q_s), (v_hbm, v_s), (x_hbm.at[:, 0:H], x_s.at[0]), (x_hbm.at[:, H:D], x_s.at[1]),
+        (o_hbm, o_s),
         (wg_hbm, wg_s), (wu_hbm, wu_s), (wd_hbm, wd_s), (wo_hbm, wo_s),
     ]
     loads = [pltpu.make_async_copy(a, b, lsem.at[i]) for i, (a, b) in enumerate(loads)]
@@ -109,20 +112,6 @@
     weight_hi = weight.astype(BF16)
     weight_lo = (weight - weight_hi.astype(F32)).astype(BF16)
 
-    loads[0].wait()
-    loads[1].wait()
-    gain_half = fgain_ref[:, pl.ds(pl.multiple_of(c * H, 128), H)]
-
-    def norm_rows(i, carry):
-        rows = pl.ds(pl.multiple_of(i * 64, 64), 64)
-        a, b = x_s[0, rows, :].astype(F32), x_s[1, rows, :].astype(F32)
-        total = jnp.sum(a * a + b * b, axis=-1, keepdims=True)
-        factor = lax.rsqrt(total / D + EPS)
-        n_s[rows, :] = (x_s[c, rows, :].astype(F32) * factor * gain_half).astype(BF16)
-        return carry
-
-    lax.fori_loop(0, NTOK // 64, norm_rows, 0)
-
     place_row = lax.broadcasted_iota(jnp.int32, (KR, NTOK), 0).astype(F32)
 
     def fill_group(g):
@@ -131,32 +120,31 @@
             g_s[rows, :] = jnp.where(place_row == slot_s[k : k + 1, :], 1.0, 0.0).astype(BF16)
         rows = slice(g * GR, (g + 1) * GR)
         pick = g_s[rows, :]
-        for n in range(0, H, 256):
-            s_s[rows, n : n + 256] = jnp.dot(
-                pick, n_s[:, n : n + 256], preferred_element_type=F32
+        for n in range(0, H, min(HW, 256)):
+            at = n % HW
+            s_s[n // HW, rows, at : at + min(HW, 256)] = jnp.dot(
+                pick, n_s[:, n : n + min(HW, 256)], preferred_element_type=F32
             ).astype(BF16)
 
-    def dispatch(k):
+    def dispatch(w, k):
         rows = slice(k * KR, (k + 1) * KR)
         return remote(
-            s_s.at[rows, :], r_s.at[c, rows, :], asend.at[k], arecv.at[k], moved(me, offs[k], E), t
-        )
-
-    def forward(k):
-        rows = slice(k * KR, (k + 1) * KR)
+            s_s.at[w, rows, :], r_s.at[c, w, rows, :], asend.at[w, k], arecv.at[w, k],
+            moved(me, offs[k], E), t,
+        )
+
+    def forward(w, g, core):
+        rows = slice(g * GR, (g + 1) * GR)
         return remote(
-            r_s.at[c, rows, :], r_s.at[c, rows, :], fsend.at[k], frecv.at[k], me, z * 2 + pc
-        )
-
-    fill_group(0)
-    r_s[c, 0:KR, :] = s_s[0:KR, :]
+            r_s.at[core, w, rows, :], r_s.at[core, w, rows, :], fsend.at[w, g], frecv.at[w, g], me, z * 2 + pc
+        )
 
     ta = lax.broadcasted_iota(jnp.int32, (PAIR, PAIR), 0)
     tb = lax.broadcasted_iota(jnp.int32, (PAIR, PAIR), 1)
     tri = (ta // BLOCK == tb // BLOCK) & (ta >= tb)
     tri_s[...] = jnp.where(tri, 1.0, 0.0)
     gap = gap_ref[...]
-    for load in loads[2:6]:
+    for load in loads[0:3]:
         load.wait()
     U1 = min(4, TOK // PAIR)
 
@@ -240,24 +228,29 @@
     pl.semaphore_wait(barrier, E - 1 + 3)
     for k in range(1, E):
         hand_on(k).start()
-    for k in range(1, KG):
-        dispatch(k).start()
-    for g in range(1, NG):
+
+    loads[3].wait()
+    loads[4].wait()
+    gain_half = fgain_ref[:, pl.ds(pl.multiple_of(c * H, 128), H)]
+
+    def norm_rows(i, carry):
+        rows = pl.ds(pl.multiple_of(i * 64, 64), 64)
+        a, b = x_s[0, rows, :].astype(F32), x_s[1, rows, :].astype(F32)
+        total = jnp.sum(a * a + b * b, axis=-1, keepdims=True)
+        factor = lax.rsqrt(total / D + EPS)
+        n_s[rows, :] = (x_s[c, rows, :].astype(F32) * factor * gain_half).astype(BF16)
+        return carry
+
+    lax.fori_loop(0, NTOK // 64, norm_rows, 0)
+
+    for g in range(NG):
         fill_group(g)
-        for k in range(g * KG, (g + 1) * KG):
-            dispatch(k).start()
-
-    def swapper(ref, outer, inner):
-        size = outer * inner * UNIT
-        row = lax.broadcasted_iota(jnp.int32, (size, 1), 0)
-        source = (row // UNIT % inner * outer + row // (inner * UNIT)) * UNIT + row % UNIT
-        ref[...] = jnp.where(lax.broadcasted_iota(jnp.int32, (size, size), 1) == source, 1.0, 0.0).astype(BF16)
-
-    swapper(perm_s, Z, SG)
-    swapper(perm_back_s, SG, J)
-
+    r_s[c, :, 0:KR, :] = s_s[:, 0:KR, :]
     for k in range(1, E):
         handed(k).wait_recv()
+    for k in range(1, E):
+        dispatch(0, k).start()
+
     start = jnp.zeros((VAL_DIM, KEY_DIM), F32)
     for j in range(E - 1):
         ends = cr_s[j, VAL_DIM : VAL_DIM + 16, :].astype(F32)
@@ -267,6 +260,8 @@
     gb = lax.broadcasted_iota(jnp.int32, (VAL_DIM, VAL_DIM), 1)
     head_gain = jnp.sum(jnp.where(ga == gb, hgain_ref[...], 0.0), axis=-1, keepdims=True)
     own_rows = pl.multiple_of(t * VAL_DIM, VAL_DIM)
+
+    loads[5].wait()
 
     def finish_pairs(i, carry):
         left = lax.broadcasted_iota(jnp.int32, (BLOCK, PAIR), 1) < BLOCK
@@ -336,27 +331,40 @@
             ring(way, half, 1).start()
     share(0, c).start()
 
-    def forward_group(g):
+    def swapper(ref, outer, inner):
+        size = outer * inner * UNIT
+        row = lax.broadcasted_iota(jnp.int32, (size, 1), 0)
+        source = (row // UNIT % inner * outer + row // (inner * UNIT)) * UNIT + row % UNIT
+        ref[...] = jnp.where(lax.broadcasted_iota(jnp.int32, (size, size), 1) == source, 1.0, 0.0).astype(BF16)
+
+    swapper(perm_s, Z, SG)
+    swapper(perm_back_s, SG, J)
+
+    def forward_group(w, g):
         for k in range(g * KG, (g + 1) * KG):
             if k:
-                dispatch(k).wait_recv()
-            forward(k).start()
-
-    def ffn(g):
+                dispatch(w, k).wait_recv()
+        forward(w, g, c).start()
+
+    def ffn(w, g):
         rows = slice(g * GR, (g + 1) * GR)
-        for k in range(g * KG, (g + 1) * KG):
-            back = slice(k * KR, (k + 1) * KR)
-            remote(
-                r_s.at[c, back, :], r_s.at[pc, back, :], fsend.at[k], frecv.at[k], me, z * 2 + pc
-            ).wait_recv()
-        a, b = r_s[0, rows, :], r_s[1, rows, :]
-        gate = lax.dot_general(a, wg_s[:, 0:H], NT, preferred_element_type=F32) + lax.dot_general(
-            b, wg_s[:, H:D], NT, preferred_element_type=F32
-        )
-        up = lax.dot_general(a, wu_s[:, 0:H], NT, preferred_element_type=F32) + lax.dot_general(
-            b, wu_s[:, H:D], NT, preferred_element_type=F32
-        )
-        hid_s[rows, :] = (gate * (1.0 / (1.0 + jnp.exp(-gate))) * up).astype(BF16)
+        forward(w, g, pc).wait_recv()
+        a, b = r_s[0, w, rows, :], r_s[1, w, rows, :]
+        ca, cb = slice(w * HW, (w + 1) * HW), slice(H + w * HW, H + (w + 1) * HW)
+
+        def product(weight):
+            return lax.dot_general(a, weight[:, ca], NT, preferred_element_type=F32) + lax.dot_general(
+                b, weight[:, cb], NT, preferred_element_type=F32
+            )
+
+        gate, up = product(wg_s), product(wu_s)
+        if w:
+            gate, up = gate + ga_s[rows, :], up + ua_s[rows, :]
+        if w < NW - 1:
+            ga_s[rows, :] = gate
+            ua_s[rows, :] = up
+        else:
+            hid_s[rows, :] = (gate * (1.0 / (1.0 + jnp.exp(-gate))) * up).astype(BF16)
 
     def relative(r):
         return lax.rem(z + r + 2 * Z, Z)
@@ -368,8 +376,11 @@
             me, z * 2 + pc,
         )
 
+    def way_of(d):
+        return 1 - 2 * (d % 2)
+
     def pass_on(g, d, s):
-        way = 1 - 2 * d
+        way = way_of(d)
         part = relative(-way * (1 + s))
         return remote(
             pp_s.at[c, d, g, part], rb_s.at[s, g, d], bsend.at[s, g, d], brecv.at[s, g, d],
@@ -379,7 +390,7 @@
     swapped = set()
 
     def add_and_pass(g, d, s):
-        r = -(1 - 2 * d) * (1 + s)
+        r = -way_of(d) * (1 + s)
         part = relative(r)
         if (g, r % Z) not in swapped:
             swapped.add((g, r % Z))
@@ -412,7 +423,7 @@
                 axis=0,
             )
             for half in range(2):
-                for d in range(2):
+                for d in range(ND):
                     cols = slice(half * H + d * W, half * H + (d + 1) * W)
                     y = jnp.dot(hid, wd_s[:, cols], preferred_element_type=F32).astype(BF16)
                     for i, r in enumerate(pair):
@@ -420,25 +431,45 @@
             for r in pair:
                 swap(g, r).start()
             if n == min(2, Z - 2):
-                for d in range(2):
+                for d in range(ND):
                     add_and_pass(g, d, 0)
 
     hops = max(reach.values())
     for load in loads[6:]:
         load.wait()
-    forward_group(0)
-    done = 0
-    for g in range(NG):
-        ffn(g)
+    half = NG // 2
+    todo = list(range(1, hops + 1))
+
+    def next_hop():
+        if todo:
+            relay(todo.pop(0))
+
+    next_hop()
+    for w in range(1, NW):
+        for k in range(1, E):
+            dispatch(w, k).start()
+        for g in range(NG):
+            forward_group(w - 1, g)
+        next_hop()
+        for g in range(NG):
+            ffn(w - 1, g)
+    while todo:
+        next_hop()
+    forward_group(NW - 1, 0)
+    for g in range(half):
+        forward_group(NW - 1, g + 1)
+        ffn(NW - 1, g)
+    down(0)
+    for g in range(half, NG):
         if g + 1 < NG:
-            forward_group(g + 1)
-        if g + 1 <= hops:
-            relay(g + 1)
-        while done < NS and (done + 1) * SG <= (g + 1) * KG:
-            down(done)
-            done += 1
-    for hop in range(NG + 1, hops + 1):
-        relay(hop)
+            forward_group(NW - 1, g + 1)
+        ffn(NW - 1, g)
+    ahead = 1 if Z > 2 else 0
+    if ahead:
+        for d in range(ND):
+            add_and_pass(0, d, ahead)
+    if NS > 1:
+        down(1)
 
     out_copy = pltpu.make_async_copy(out_s, out_hbm, osem)
 
@@ -483,18 +514,21 @@
         )
 
     side = [functools.partial(project, n) for n in range(4)] + [weigh_all]
+    def last(g):
+        rows = slice(g * SG * BR, (g + 1) * SG * BR)
+        fb_s[rows, :] = jnp.dot(perm_back_s[...], fs_s[g], preferred_element_type=F32).astype(BF16)
+        for k in range(g * SG, (g + 1) * SG):
+            if k:
+                give_back(k).start()
+
     for s in range(1, Z):
-        for g in range(NS):
-            for d in range(2):
-                add_and_pass(g, d, s)
-            if s == Z - 1:
-                rows = slice(g * SG * BR, (g + 1) * SG * BR)
-                fb_s[rows, :] = jnp.dot(
-                    perm_back_s[...], fs_s[g], preferred_element_type=F32
-                ).astype(BF16)
-                for k in range(g * SG, (g + 1) * SG):
-                    if k:
-                        give_back(k).start()
+        for g in reversed(range(NS)):
+            step = s if g else s + ahead
+            if step < Z:
+                for d in range(ND):
+                    add_and_pass(g, d, step)
+            if step == Z - 1:
+                last(g)
         if s < Z - 1:
             for _ in range(-(-len(side) // max(1, Z - 1 - s))):
                 side.pop(0)()
@@ -523,11 +557,13 @@
             moe_ref[:, half * H + j * 128 : half * H + (j + 1) * 128] = mo_s[half, j]
 
     for k in range(1, E):
-        dispatch(k).wait_send()
+        for w in range(NW):
+            dispatch(w, k).wait_send()
         hand_on(k).wait_send()
         give_back(k).wait_send()
-    for k in range(E):
-        forward(k).wait_send()
+    for w in range(NW):
+        for g in range(NG):
+            forward(w, g, c).wait_send()
     for way, half in lanes:
         for hop in range(1, reach[way, half] + 1):
             ring(way, half, hop).wait_send()
@@ -536,7 +572,7 @@
     for g in range(NS):
         for r in range(Z):
             swap(g, r).wait_send()
-        for d in range(2):
+        for d in range(ND):
             for s in range(Z - 1):
                 pass_on(g, d, s).wait_send()
     hand_over(c).wait_send()
@@ -559,8 +595,11 @@
     SG = max(1, E // 2)
     NS, UNIT, J = E // SG, 2 * CAP, H // 128
     SR = SG * UNIT
-    cfg = dict(E=E, TP=TP, TOK=TOK, SUB=SUB, CAP=CAP)
+    ND = 4 if H % 512 == 0 else 2
+    NW = 2
+    cfg = dict(E=E, TP=TP, TOK=TOK, SUB=SUB, CAP=CAP, ND=ND, NW=NW)
     any_spec = pl.BlockSpec(memory_space=pl.ANY)
+    hbm = pl.BlockSpec(memory_space=pl.ANY)
     vmem = pl.BlockSpec(memory_space=pltpu.VMEM)
     dma = pltpu.SemaphoreType.DMA
     V = pltpu.VMEM
@@ -571,7 +610,7 @@
             jax.ShapeDtypeStruct((TOK, w_out.shape[1]), BF16),
             jax.ShapeDtypeStruct((SUB, D), BF16),
         ),
-        in_specs=[any_spec] * 4 + [vmem] * 3 + [any_spec] * 2 + [vmem] * 3 + [any_spec] * 3,
+        in_specs=[hbm] * 4 + [vmem] * 3 + [hbm] * 2 + [vmem] * 3 + [hbm] * 3,
         out_specs=(any_spec, vmem),
         scratch_shapes=[
             V((TOK, KEY_DIM), BF16), V((TOK, KEY_DIM), BF16), V((VAL_DIM, TOK), BF16), V((VAL_DIM, TOK), BF16),
@@ -579,17 +618,19 @@
             V((PAIR, PAIR), F32), V((TOK // PAIR * 8, KEY_DIM), F32), V((TOK, KEY_DIM), F32),
             V((VAL_DIM, TOK), F32), V((TOK, KEY_DIM), BF16), V((VAL_DIM + 16, KEY_DIM), BF16),
             V((E, VAL_DIM + 16, KEY_DIM), BF16),
-            V((NTOK, H), BF16), V((E, NTOK), F32), V((ROWS, NTOK), BF16), V((ROWS, H), BF16),
-            V((2, ROWS, H), BF16), V((ROWS, FF), BF16), V((ROWS, FF), BF16),
-            V((2, 2, NS, Z, SR, H // 2), BF16), V((2, NS, Z, SR, H // 2), BF16), V((Z - 1, NS, 2, SR, H // 2), BF16),
+            V((NTOK, H), BF16), V((E, NTOK), F32), V((ROWS, NTOK), BF16), V((NW, ROWS, H // NW), BF16),
+            V((2, NW, ROWS, H // NW), BF16), V((ROWS, FF), F32), V((ROWS, FF), F32),
+            V((ROWS, FF), BF16), V((ROWS, FF), BF16),
+            V((2, ND, NS, Z, SR, H // ND), BF16), V((ND, NS, Z, SR, H // ND), BF16),
+            V((Z - 1, NS, ND, SR, H // ND), BF16),
             V((Z * SR, Z * SR), BF16), V((J * SR, J * SR), BF16),
             V((TP * VAL_DIM, TOK), BF16), V((TOK, w_out.shape[1]), BF16), V((NS, J * SR, 128), BF16),
             V((E * J * UNIT, 128), BF16), V((E * J * UNIT, 128), BF16),
             V((E * J * UNIT, J * 2 * SUB), BF16), V((E * J * UNIT, J * 2 * SUB), BF16),
             V((J, 2 * SUB, 128), BF16), V((2, J, SUB, 128), BF16),
-            dma((10,)), dma, dma((E,)), dma((E,)), dma((E,)), dma((E,)), dma((E,)), dma((E,)),
+            dma((10,)), dma, dma((NW, E)), dma((NW, E)), dma((NW, NG)), dma((NW, NG)), dma((E,)), dma((E,)),
             dma((2, 2, hops)), dma((2, 2, hops)), dma((Z,)), dma((Z,)), dma((NS, Z)), dma((NS, Z)),
-            dma((Z - 1, NS, 2)), dma((Z - 1, NS, 2)), dma((E,)), dma((E,)), dma, dma,
+            dma((Z - 1, NS, ND)), dma((Z - 1, NS, ND)), dma((E,)), dma((E,)), dma, dma,
         ],
         compiler_params=pltpu.CompilerParams(
             collective_id=0, has_side_effects=True, vmem_limit_bytes=64000 * 1024

time: 107 us -> 102 us (0.953)
  Pallas kernels: 103 us -> 97.7 us
    pallas_call x1, Pallas kernels: 103 us -> 97.7 us  [on_device(): pl.pallas_call(functools.partial(kernel, cfg), out_shape=(jax.ShapeDtypeS...]
where the time goes in v3:
time: 102 us
  Pallas kernels  97.7 us (96%)
  local copies, waits for them, and re-layouts  3.44 us (3%)
    pallas_call x1, Pallas kernels, on_device(): pl.pallas_call(functools.partial(kernel, cfg), out_shape=(jax.ShapeDtypeS...  97.7 us
    unnamed x2, local copies, waits for them, and re-layouts  3.44 us

profile of v3, /device:TPU:1, one launch (start us, length us, event | category | flops | bytes accessed | tf_op | source)
XLA Modules:
  0.0 101.8 jit_solution(15811302861274637628)
XLA Ops:
  0.6 97.7 %shard_map.158 = (bf16[2048,128]{1,0:T(8,128)(2,1)}, bf16[32,2048]{1,0:T(8,128)(2,1)}) custom-call(bf16[2048,128]{1,0:T(8,128)(2,1)} %q_hbm.1, bf16[2048,128]{1,0:T(8,128)(2,1)} %f_hbm.1, bf16[64,2048]{1,0:T(8,128)(2,1)} %bitcast.18, bf16[64,2048]{1,0:T(8,128)(2,1)} %bitcast.19, f32[1,128]{1,0:T(1,128)} %bitcast.24, f32[1,2048]{1,0:T(1,128)} %bitcast.20, ...), custom_call_target="tpu_custom_call" | custom-call | tf_op jit(solution)/shard_map/pallas_call | solution.py:607
  98.4 1.9 %copy.19 = bf16[2048,128]{1,0:T(8,128)(2,1)} copy(bf16[2048,128]{1,0:T(8,128)(2,1)} %get-tuple-element.4) | data formatting | bytes 1048576
  100.2 1.6 %copy.20 = bf16[32,2048]{1,0:T(8,128)(2,1)} copy(bf16[32,2048]{1,0:T(8,128)(2,1)} %get-tuple-element.5) | data formatting | bytes 262144

commit v4 on v3

--- a/solution.py
+++ b/solution.py
@@ -407,7 +407,7 @@
                 at = (d * (W // 128) + n) * SR
                 fs_s[g, at : at + SR, :] = total[:, n * 128 : n * 128 + 128].astype(BF16)
 
-    def down(g):
+    def down(g, between=None):
         rows = slice(g * Z * SR, (g + 1) * Z * SR)
         hp_s[rows, :] = jnp.dot(
             perm_s[...], hid_s[rows, :], preferred_element_type=F32
@@ -430,6 +430,8 @@
                         pp_s[half, d, g, relative(r)] = y[i * SR : (i + 1) * SR, :]
             for r in pair:
                 swap(g, r).start()
+            if between and n == 2:
+                between()
             if n == min(2, Z - 2):
                 for d in range(ND):
                     add_and_pass(g, d, 0)
@@ -579,6 +581,18 @@
     out_copy.wait()
 
 
+def settle(a_in, b_in, a_out, b_out, a_s, b_s, sem):
+    ins = [pltpu.make_async_copy(a_in, a_s, sem.at[0]), pltpu.make_async_copy(b_in, b_s, sem.at[1])]
+    outs = [pltpu.make_async_copy(a_s, a_out, sem.at[2]), pltpu.make_async_copy(b_s, b_out, sem.at[3])]
+    for copy in ins:
+        copy.start()
+    for copy, out in zip(ins, outs):
+        copy.wait()
+        out.start()
+    for out in outs:
+        out.wait()
+
+
 def on_device(
     query, forget, values, out_gate, gap, extra, head_gain, w_out,
     tokens, ff_gain, chosen, chosen_w, w_gate, w_up, w_down,
@@ -604,7 +618,7 @@
     dma = pltpu.SemaphoreType.DMA
     V = pltpu.VMEM
     hops = Z // 2
-    return pl.pallas_call(
+    results = pl.pallas_call(
         functools.partial(kernel, cfg),
         out_shape=(
             jax.ShapeDtypeStruct((TOK, w_out.shape[1]), BF16),
@@ -639,6 +653,13 @@
         query, forget, values.T, out_gate.T, gap.reshape(1, -1), extra.T, head_gain.reshape(1, -1), w_out,
         tokens, ff_gain.reshape(1, -1), chosen.T, chosen_w.T, w_gate[0].T, w_up[0].T, w_down[0],
     )
+    return pl.pallas_call(
+        settle,
+        out_shape=tuple(jax.ShapeDtypeStruct(r.shape, r.dtype) for r in results),
+        in_specs=[any_spec] * 2,
+        out_specs=(any_spec, any_spec),
+        scratch_shapes=[V(results[0].shape, BF16), V(results[1].shape, BF16), dma((4,))],
+    )(*results)
 
 
 def solution(mesh):

time: 102 us -> 101 us (level)
  local copies, waits for them, and re-layouts: 3.44 us -> 0 us
  Pallas kernels: 97.7 us -> 99.6 us
    unnamed x2 -> x0, local copies, waits for them, and re-layouts: 3.44 us -> none
    pallas_call x0 -> x1, Pallas kernels: none -> 1.9 us  [on_device(): pl.pallas_call(settle, out_shape=tuple((jax.ShapeDtypeStruct(r.shape, r.d...]
where the time goes in v4:
time: 101 us; the launch traced here: 100 us
  Pallas kernels  99.6 us (99%)
    pallas_call x1, Pallas kernels, on_device(): pl.pallas_call(functools.partial(kernel, cfg), out_shape=(jax.ShapeDtypeS...  97.7 us

profile of v4, /device:TPU:1, one launch (start us, length us, event | category | flops | bytes accessed | tf_op | source)
XLA Modules:
  0.0 100.4 jit_solution(15443408354114348979)
XLA Ops:
  0.6 97.7 %shard_map.158 = (bf16[2048,128]{1,0:T(8,128)(2,1)}, bf16[32,2048]{1,0:T(8,128)(2,1)}) custom-call(bf16[2048,128]{1,0:T(8,128)(2,1)} %q_hbm.1, bf16[2048,128]{1,0:T(8,128)(2,1)} %f_hbm.1, bf16[64,2048]{1,0:T(8,128)(2,1)} %bitcast.18, bf16[64,2048]{1,0:T(8,128)(2,1)} %bitcast.19, f32[1,128]{1,0:T(1,128)} %bitcast.24, f32[1,2048]{1,0:T(1,128)} %bitcast.20, ...), custom_call_target="tpu_custom_call" | custom-call | tf_op jit(solution)/shard_map/pallas_call | solution.py:621
  98.4 1.9 %shard_map.159 = (bf16[2048,128]{1,0:T(8,128)(2,1)}, bf16[32,2048]{1,0:T(8,128)(2,1)}) custom-call(bf16[2048,128]{1,0:T(8,128)(2,1)} %get-tuple-element.4.a_in, bf16[32,2048]{1,0:T(8,128)(2,1)} %get-tuple-element.5.b_in), custom_call_target="tpu_custom_call" | custom-call | tf_op jit(solution)/shard_map/pallas_call | solution.py:656

commit v5 on v4

--- a/solution.py
+++ b/solution.py
@@ -227,7 +227,7 @@
 
     pl.semaphore_wait(barrier, E - 1 + 3)
     for k in range(1, E):
-        hand_on(k).start()
+        pl.when(moved(me, offs[k], E) > me)(hand_on(k).start)
 
     loads[3].wait()
     loads[4].wait()
@@ -247,7 +247,7 @@
         fill_group(g)
     r_s[c, :, 0:KR, :] = s_s[:, 0:KR, :]
     for k in range(1, E):
-        handed(k).wait_recv()
+        pl.when(moved(me, offs[k], E, back=True) < me)(handed(k).wait_recv)
     for k in range(1, E):
         dispatch(0, k).start()
 
@@ -561,7 +561,7 @@
     for k in range(1, E):
         for w in range(NW):
             dispatch(w, k).wait_send()
-        hand_on(k).wait_send()
+        pl.when(moved(me, offs[k], E) > me)(hand_on(k).wait_send)
         give_back(k).wait_send()
     for w in range(NW):
         for g in range(NG):

time: 101 us -> 106 us (1.050)
  Pallas kernels: 99.6 us -> 105 us
    pallas_call x1, Pallas kernels: 97.7 us -> 103 us  [on_device(): pl.pallas_call(functools.partial(kernel, cfg), out_shape=(jax.ShapeDtypeS...]
where the time goes in v5:
time: 106 us
  Pallas kernels  105 us (99%)
    pallas_call x1, Pallas kernels, on_device(): pl.pallas_call(functools.partial(kernel, cfg), out_shape=(jax.ShapeDtypeS...  103 us

profile of v5, /device:TPU:1, one launch (start us, length us, event | category | flops | bytes accessed | tf_op | source)
XLA Modules:
  0.0 105.9 jit_solution(3074784647415707245)
XLA Ops:
  0.6 103.2 %shard_map.158 = (bf16[2048,128]{1,0:T(8,128)(2,1)}, bf16[32,2048]{1,0:T(8,128)(2,1)}) custom-call(bf16[2048,128]{1,0:T(8,128)(2,1)} %q_hbm.1, bf16[2048,128]{1,0:T(8,128)(2,1)} %f_hbm.1, bf16[64,2048]{1,0:T(8,128)(2,1)} %bitcast.18, bf16[64,2048]{1,0:T(8,128)(2,1)} %bitcast.19, f32[1,128]{1,0:T(1,128)} %bitcast.24, f32[1,2048]{1,0:T(1,128)} %bitcast.20, ...), custom_call_target="tpu_custom_call" | custom-call | tf_op jit(solution)/shard_map/pallas_call | solution.py:621
  103.9 1.9 %shard_map.159 = (bf16[2048,128]{1,0:T(8,128)(2,1)}, bf16[32,2048]{1,0:T(8,128)(2,1)}) custom-call(bf16[2048,128]{1,0:T(8,128)(2,1)} %get-tuple-element.4.a_in, bf16[32,2048]{1,0:T(8,128)(2,1)} %get-tuple-element.5.b_in), custom_call_target="tpu_custom_call" | custom-call | tf_op jit(solution)/shard_map/pallas_call | solution.py:656
